TPU v7x, 32 devices: a whole 2x2x4 slice. The times are simulated.
32 devices in a mesh: sp: 8 (over z, x), tp: 4 (over y, core).
Axes of the slice: x: 2, y: 2, z: 4, core: 2. Of those that a mesh axis runs over, the one named last changes fastest.
Arguments:
- tokens: bfloat16 [2048, 4096], P(('sp', 'tp')), may hold values from -40 to 40, as said below
- query_weight: bfloat16 [2, 4096, 4096], P(None, 'sp', 'tp'), may hold values from -0.09375 to 0.09375
- key_weight: bfloat16 [2, 4096, 512], P(None, 'sp', 'tp'), may hold values from -0.09375 to 0.09375
- value_weight: bfloat16 [2, 4096, 512], P(None, 'sp', 'tp'), may hold values from -0.09375 to 0.09375
- gate_weight: bfloat16 [2, 4096, 4096], P(None, 'sp', 'tp'), may hold values from -0.09375 to 0.09375
- out_weight: bfloat16 [2, 4096, 4096], P(None, 'tp', 'sp'), may hold values from -0.09375 to 0.09375
- sink_logits: float32 [2, 64], replicated, may hold values from 1 to 6
- out_gain: float32 [2, 4096], replicated, may hold values from 0.1 to 1.9
Outputs:
- current: float32 [2048, 4096], P(('sp', 'tp'))
Inputs may be any that keep to these rules, and one draw needn't show every extreme that they name: tokens are finite and within -40 to 40.
All inputs are finite; a program needn't handle non-finite values.
Results may differ from a plain program's by a relative error of at most 0.014.
The roundings to bfloat16 on the way count: a program that leaves them out, or rounds other values in their place, can miss the bound.
Values may be sent and summed in bfloat16 or wider, within the bound.
A program may use at most 128 MiB of HBM per device.

v0:
```python
import jax
import jax.numpy as jnp
from jax import lax
from jax.sharding import PartitionSpec as P

HEAD_DIM = 64
WINDOW = 128
LAYERS = 2


norm_epsilon = 1e-05
masked_score = -1e30


def shifted(value, axis, by):
    length = lax.axis_size(axis)
    pairs = [(i, i + by) for i in range(length) if 0 <= i + by < length]
    return lax.ppermute(value, axis, pairs)


def per_device(
    tokens, query_weight, key_weight, value_weight, gate_weight, out_weight, sink_logits, out_gain
):
    tp_count = lax.axis_size("tp")
    rows_here = tokens.shape[0]
    seq_rows = rows_here * tp_count
    query_cols = query_weight.shape[2]
    key_cols = key_weight.shape[2]
    heads_here = query_cols // HEAD_DIM
    kv_here = key_cols // HEAD_DIM
    group_size = heads_here // kv_here
    block_start = lax.axis_index("sp") * seq_rows
    head_start = lax.axis_index("tp") * heads_here
    query_pos = block_start + jnp.arange(seq_rows)
    key_pos = block_start - WINDOW + jnp.arange(WINDOW + seq_rows)
    distance = query_pos[:, None] - key_pos[None, :]
    visible = (distance >= 0) & (distance < WINDOW) & (key_pos >= 0)[None, :]
    score_scale = HEAD_DIM ** (-0.5)
    current = tokens
    result = None
    for depth_index in range(LAYERS):
        joined = jnp.concatenate(
            [
                query_weight[depth_index],
                gate_weight[depth_index],
                key_weight[depth_index],
                value_weight[depth_index],
            ],
            axis=1,
        )
        gathered = lax.all_gather(current, "tp", axis=0, tiled=True)
        projected = jnp.dot(
            gathered,
            lax.all_gather(joined, "sp", axis=0, tiled=True),
            preferred_element_type=jnp.float32,
        ).astype(jnp.bfloat16)
        own_keys = projected[:, 2 * query_cols :]
        before = shifted(own_keys[-WINDOW:], "sp", 1)
        nearby = jnp.concatenate([before, own_keys], axis=0)
        queries = projected[:, :query_cols].reshape(seq_rows, kv_here, group_size, HEAD_DIM)
        gate_part = projected[:, query_cols : 2 * query_cols]
        key_part = nearby[:, :key_cols].reshape(WINDOW + seq_rows, kv_here, HEAD_DIM)
        value_part = nearby[:, key_cols:].reshape(WINDOW + seq_rows, kv_here, HEAD_DIM)
        scores = (
            jnp.einsum("qhgd,khd->hgqk", queries, key_part, preferred_element_type=jnp.float32)
            * score_scale
        )
        scores = jnp.where(visible[None, None], scores, masked_score)
        sink_here = lax.dynamic_slice_in_dim(sink_logits[depth_index], head_start, heads_here, 0)
        sink_part = sink_here.reshape(kv_here, group_size, 1, 1)
        highest = jnp.maximum(jnp.max(scores, axis=-1, keepdims=True), sink_part)
        exponent = jnp.exp(scores - highest)
        weights = (
            exponent / (jnp.sum(exponent, axis=-1, keepdims=True) + jnp.exp(sink_part - highest))
        ).astype(jnp.bfloat16)
        mixture = jnp.einsum(
            "hgqk,khd->qhgd", weights, value_part, preferred_element_type=jnp.float32
        )
        mixture = mixture.reshape(seq_rows, query_cols)
        hidden = (mixture * jax.nn.silu(gate_part.astype(jnp.float32))).astype(jnp.bfloat16)
        partial_value = jnp.dot(
            hidden,
            lax.all_gather(out_weight[depth_index], "sp", axis=1, tiled=True),
            preferred_element_type=jnp.float32,
        )
        summed = lax.psum_scatter(partial_value, "tp", scatter_dimension=0, tiled=True)
        factor = lax.rsqrt(jnp.mean(summed * summed, axis=-1, keepdims=True) + norm_epsilon)
        result = summed * factor * out_gain[depth_index]
        current = result.astype(jnp.bfloat16)
    return result


def solution(mesh):
    placed = (
        P(("sp", "tp"), None),
        P(None, "sp", "tp"),
        P(None, "sp", "tp"),
        P(None, "sp", "tp"),
        P(None, "sp", "tp"),
        P(None, "tp", "sp"),
        P(),
        P(),
    )
    return jax.shard_map(
        per_device, mesh=mesh, in_specs=placed, out_specs=P(("sp", "tp"), None), check_vma=False
    )
```

profile of v0, /device:TPU:9, one launch (start us, length us, event | category | flops | bytes accessed | tf_op | source)
XLA Modules:
  0.0 1154.3 jit_solution(12527978548240148429)
XLA Ops:
  6.5 0.0 all-gather.11.cloned.1.call-start
  6.5 0.7 all-gather.11.cloned.1.call-update
  7.3 0.0 all-gather.9.cloned.1.call-start
  7.3 1.8 slice_bitcast_fusion.4
  9.1 2.7 slice_bitcast_fusion
  11.8 1.6 pad_maximum_fusion
  13.4 0.0 all-gather.9.cloned.1.call-update
  13.4 0.0 all-gather.17.cloned.1.call-start
  13.5 3.1 fusion.29
  16.5 0.0 all-gather.17.cloned.1.call-update
  16.6 0.0 reduce-scatter.3.cloned.1.call-start
  16.7 0.2 fusion.22
  16.8 0.0 copy-start.3
  16.8 16.2 %all-gather.11.cloned.1.call-done = bf16[256,4096]{1,0:T(8,128)(2,1)} async-done(((bf16[64,4096]{1,0:T(8,128)(2,1)}), bf16[256,4096]{1,0:T(8,128)(2,1)}) %all-gather.11.cloned.1.call-update) | async-done | bytes 2097168 | tf_op jit(solution)/shard_map/all_gather | solution.py:51
  33.0 363.7 %all-gather.9.cloned.1.call-done = bf16[4096,2304]{1,0:T(8,128)(2,1)} async-done(((bf16[512,2304]{1,0:T(8,128)(2,1)}), bf16[4096,2304]{1,0:T(8,128)(2,1)}) %all-gather.9.cloned.1.call-update) | async-done | bytes 18874384 | tf_op jit(solution)/shard_map/all_gather | solution.py:54
  396.7 9.6 fusion.8
  406.4 0.0 copy-start
  406.4 0.7 slice.106
  407.1 1.9 collective-permute-start
  409.0 0.0 copy-done.3
  409.0 0.1 dynamic-slice_reduce_fusion
  409.1 0.1 max.36
  409.3 6.3 collective-permute-done
  415.5 0.8 pad_maximum_fusion.3
  416.3 1.1 fusion.6
  417.4 0.1 broadcast_maximum_fusion.1
  417.5 1.3 fusion.4
  418.8 0.0 copy-done
  418.8 0.1 exponential_add_fusion.1
  418.9 1.9 fusion.9
  420.8 1.5 fusion.20
  422.3 0.0 copy-start.1
  422.3 100.8 %all-gather.17.cloned.1.call-done = bf16[1,1024,4096]{2,1,0:T(8,128)(2,1)} async-done(((bf16[1,1024,512]{2,1,0:T(8,128)(2,1)}), bf16[1,1024,4096]{2,1,0:T(8,128)(2,1)}) %all-gather.17.cloned.1.call-update) | async-done | bytes 8388624 | tf_op jit(solution)/shard_map/all_gather | solution.py:83
  523.0 7.8 fusion.2
  530.8 0.0 reduce-scatter.3.cloned.1.call-update
  530.9 0.0 all-gather.15.cloned.1.call-start
  530.9 1.5 pad_maximum_fusion.1
  532.5 0.0 all-gather.15.cloned.1.call-update
  532.5 0.0 all-gather.13.cloned.1.call-start
  532.6 43.6 %reduce-scatter.3.cloned.1.call-done = f32[64,4096]{1,0:T(8,128)} async-done(((f32[256,4096]{1,0:T(8,128)}), f32[64,4096]{1,0:T(8,128)}) %reduce-scatter.3.cloned.1.call-update) | async-done | bytes 1048592 | tf_op jit(solution)/shard_map/reduce_scatter | solution.py:86
  576.2 1.4 multiply_reduce_fusion.1
  577.6 2.2 multiply_convert_fusion
  579.8 0.0 all-gather.13.cloned.1.call-update
  579.8 0.0 all-gather.19.cloned.1.call-start
  579.9 0.7 all-gather.19.cloned.1.call-update
  580.6 0.2 reduce-scatter.5.cloned.1.call-start
  580.8 359.5 %all-gather.15.cloned.1.call-done = bf16[4096,2304]{1,0:T(8,128)(2,1)} async-done(((bf16[512,2304]{1,0:T(8,128)(2,1)}), bf16[4096,2304]{1,0:T(8,128)(2,1)}) %all-gather.15.cloned.1.call-update) | async-done | bytes 18874384 | tf_op jit(solution)/shard_map/all_gather | solution.py:54
  940.3 24.2 %all-gather.13.cloned.1.call-done = bf16[256,4096]{1,0:T(8,128)(2,1)} async-done(((bf16[64,4096]{1,0:T(8,128)(2,1)}), bf16[256,4096]{1,0:T(8,128)(2,1)}) %all-gather.13.cloned.1.call-update) | async-done | bytes 2097168 | tf_op jit(solution)/shard_map/all_gather | solution.py:51
  964.5 12.0 %convolution_convert_fusion = bf16[256,2304]{0,1:T(8,128)(2,1)S(1)} fusion(bf16[256,4096]{1,0:T(8,128)(2,1)} %all-gather.13.cloned.1.call-done, bf16[4096,2304]{1,0:T(8,128)(2,1)} %all-gather.15.cloned.1.call-done), kind=kOutput, calls=%fused_computation.14 | convolution fusion | flops 4832428032 | bytes 22151168 | tf_op jit(solution)/shard_map/dot_general | solution.py:52
  976.6 3.1 collective-permute-start.1
  979.7 0.1 max.39
  979.8 5.1 collective-permute-done.1
  984.9 1.1 fusion.7
  986.0 0.1 broadcast_maximum_fusion
  986.1 1.3 fusion.5
  987.4 0.1 exponential_add_fusion
  987.5 1.9 fusion.10
  989.4 0.3 fusion.19
  989.7 100.9 %all-gather.19.cloned.1.call-done = bf16[1,1024,4096]{2,1,0:T(8,128)(2,1)} async-done(((bf16[1,1024,512]{2,1,0:T(8,128)(2,1)}), bf16[1,1024,4096]{2,1,0:T(8,128)(2,1)}) %all-gather.19.cloned.1.call-update) | async-done | bytes 8388624 | tf_op jit(solution)/shard_map/all_gather | solution.py:83
  1090.7 7.7 fusion
  1098.4 0.0 reduce-scatter.5.cloned.1.call-update
  1098.4 45.3 %reduce-scatter.5.cloned.1.call-done = f32[64,4096]{1,0:T(8,128)} async-done(((f32[256,4096]{1,0:T(8,128)}), f32[64,4096]{1,0:T(8,128)}) %reduce-scatter.5.cloned.1.call-update) | async-done | bytes 1048592 | tf_op jit(solution)/shard_map/reduce_scatter | solution.py:86
  1143.7 1.4 multiply_reduce_fusion
  1145.1 2.4 multiply_multiply_fusion
  (16 shorter events, 0.2 us)
Async XLA Ops:
  6.5 26.5 %all-gather.11.cloned.1.call-start = ((), (), s32[]{:S(2)}) async-start(), calls=%async_computation.3 | async-start | bytes 2621440 | tf_op jit(solution)/shard_map/all_gather | solution.py:51
  7.3 389.5 %all-gather.9.cloned.1.call-start = ((), (), s32[]{:S(2)}) async-start(), calls=%async_computation.2 | async-start | bytes 21233664 | tf_op jit(solution)/shard_map/all_gather | solution.py:54
  13.4 509.6 %all-gather.17.cloned.1.call-start = ((), (), s32[]{:S(2)}) async-start(), calls=%async_computation.8 | async-start | bytes 9437184 | tf_op jit(solution)/shard_map/all_gather | solution.py:83
  16.6 559.6 %reduce-scatter.3.cloned.1.call-start = ((), (), s32[]{:S(2)}) async-start(), calls=%async_computation.4 | async-start | bytes 5242880 | tf_op jit(solution)/shard_map/reduce_scatter | solution.py:86
  16.8 392.2 %copy-start.3 = (f32[2,64]{1,0:T(2,128)S(1)}, f32[2,64]{1,0:T(2,128)}, u32[]{:S(2)}) copy-start(f32[2,64]{1,0:T(2,128)} %param.14) | copy-start | bytes 1540
  406.4 12.4 %copy-start = (bf16[256,2304]{0,1:T(8,128)(2,1)}, bf16[256,2304]{0,1:T(8,128)(2,1)S(1)}, u32[]{:S(2)}) copy-start(bf16[256,2304]{0,1:T(8,128)(2,1)S(1)} %fusion.8) | copy-start | bytes 3538948
  407.1 8.5 collective-permute-start
  422.3 108.6 %copy-start.1 = (bf16[512,128]{1,0:T(8,128)(2,1)S(1)}, bf16[512,128]{1,0:T(8,128)(2,1)}, u32[]{:S(2)}) copy-start(bf16[512,128]{1,0:T(8,128)(2,1)} %get-tuple-element.30) | copy-start | bytes 393220
  530.8 1.7 copy-start.2
  530.9 409.4 %all-gather.15.cloned.1.call-start = ((), (), s32[]{:S(2)}) async-start(), calls=%async_computation.6 | async-start | bytes 21233664 | tf_op jit(solution)/shard_map/all_gather | solution.py:54
  532.5 432.0 %all-gather.13.cloned.1.call-start = ((), (), s32[]{:S(2)}) async-start(), calls=%async_computation.5 | async-start | bytes 2621440 | tf_op jit(solution)/shard_map/all_gather | solution.py:51
  579.8 510.8 %all-gather.19.cloned.1.call-start = ((), (), s32[]{:S(2)}) async-start(), calls=%async_computation.9 | async-start | bytes 9437184 | tf_op jit(solution)/shard_map/all_gather | solution.py:83
  580.6 563.1 %reduce-scatter.5.cloned.1.call-start = ((), (), s32[]{:S(2)}) async-start(), calls=%async_computation.7 | async-start | bytes 5242880 | tf_op jit(solution)/shard_map/reduce_scatter | solution.py:86
  976.6 8.3 collective-permute-start.1
Sparse Core Ops, SparseCore 0:
  8.9 24.1 all-gather.10
  34.6 362.1 all-gather.8
  398.8 124.2 all-gather.16
  531.0 45.1 reduce-scatter.2
  577.6 362.6 all-gather.14
  941.7 22.7 all-gather.12
  966.6 124.0 all-gather.18
  1098.5 45.1 reduce-scatter.4
where the time goes:
time: 1160 us; the launch traced here: 1150 us
  waiting for transfers between devices  1070 us (92%)
  matrix products  43.1 us (4%)
  other arithmetic  16.2 us (1%)
  between operations  13.8 us (1%)
    all_gather x2, waiting for transfers between devices, per_device(): lax.all_gather(joined, 'sp', axis=0, tiled=True)  723 us
    all_gather x2, waiting for transfers between devices, per_device(): lax.all_gather(out_weight[depth_index], 'sp', axis=1, tiled=True)  202 us
    reduce_scatter x2, waiting for transfers between devices, per_device(): lax.psum_scatter(partial_value, 'tp', scatter_dimension=0, tiled=True)  88.9 us
    all_gather x2, waiting for transfers between devices, per_device(): gathered = lax.all_gather(current, 'tp', axis=0, tiled=True)  40.4 us
  transfers between devices with their start and end apart: 10, of which 10 were waited for; matrix products, arithmetic and copies ran while one was open for 4% of the time, Pallas kernels for 0%

commit v1 on v0

v1 whole, which is shorter than its diff:
```python
import functools

import jax
import jax.numpy as jnp
from jax import lax
from jax.experimental import pallas as pl
from jax.experimental.pallas import tpu as pltpu
from jax.sharding import PartitionSpec as P

HEAD_DIM = 64
WINDOW = 128
LAYERS = 2
GROUP = 8

norm_epsilon = 1e-05
masked_score = -1e30
MESH = pl.DeviceIdType.MESH


def place(nx, ncore):
    sp, tp = lax.axis_index("sp"), lax.axis_index("tp")
    return lax.div(sp, nx), lax.rem(sp, nx), lax.div(tp, ncore), lax.rem(tp, ncore)


def greet(peers):
    barrier = pltpu.get_barrier_semaphore()
    for peer in peers:
        pl.semaphore_signal(barrier, inc=1, device_id=peer, device_id_type=MESH)
    pl.semaphore_wait(barrier, len(peers))


def remote(src, dst, send, recv, peer):
    return pltpu.make_async_remote_copy(
        src_ref=src, dst_ref=dst, send_sem=send, recv_sem=recv, device_id=peer, device_id_type=MESH
    )


def gather_kernel(
    nz, nx, ny, nc, x_ref, a_ref, rows_ref, w_ref,
    own_sem, xz_s, xz_r, xy_s, xy_r, xc_s, xc_r, wz_s, wz_r, wx_s, wx_r,
):
    z, x, y, c = place(nx, nc)
    at = lambda zz, xx, yy, cc: (zz * nx + xx, yy * nc + cc)
    zs = [lax.rem(z + d, nz) for d in range(nz)]
    xs = [lax.rem(x + d, nx) for d in range(nx)]
    ys = [lax.rem(y + d, ny) for d in range(ny)]
    cs = [lax.rem(c + d, nc) for d in range(nc)]
    greet(
        [at(zs[d], x, y, c) for d in range(1, nz)]
        + [at(z, xs[d], y, c) for d in range(1, nx)]
        + [at(z, x, ys[d], c) for d in range(1, ny)]
        + [at(z, x, y, cs[d]) for d in range(1, nc)]
    )
    sent = []

    def go(*args):
        copy = remote(*args)
        copy.start()
        sent.append(copy)

    for d in range(1, nz):
        go(x_ref, rows_ref.at[z, y * nc + c], xz_s.at[d], xz_r.at[d], at(zs[d], x, y, c))
    for d in range(1, nz):
        go(a_ref.at[zs[d]], w_ref.at[z, x], wz_s.at[d], wz_r.at[d], at(zs[d], x, y, c))
    own_rows = pltpu.make_async_copy(x_ref, rows_ref.at[z, y * nc + c], own_sem.at[0])
    own_rows.start()
    own_w = pltpu.make_async_copy(a_ref.at[z], w_ref.at[z, x], own_sem.at[1])
    own_w.start()

    def spread_rows(src, zz, d):
        for e in range(1, ny):
            go(src, rows_ref.at[zz, y * nc + c], xy_s.at[d, e], xy_r.at[d, e], at(z, x, ys[e], c))
        for f in range(1, nc):
            go(src, rows_ref.at[zz, y * nc + c], xc_s.at[d, 0, f], xc_r.at[d, 0, f], at(z, x, y, cs[f]))

    def spread_w(src, zz, d):
        for e in range(1, nx):
            go(src, w_ref.at[zz, x], wx_s.at[d, e], wx_r.at[d, e], at(z, xs[e], y, c))

    spread_w(a_ref.at[z], z, 0)
    spread_rows(x_ref, z, 0)
    froms = [lax.rem(z - d + nz, nz) for d in range(nz)]
    for d in range(1, nz):
        block = rows_ref.at[froms[d], y * nc + c]
        remote(block, block, xz_s.at[d], xz_r.at[d], at(zs[d], x, y, c)).wait_recv()
        spread_rows(block, froms[d], d)
    for d in range(nz):
        for e in range(1, ny):
            yy = lax.rem(y - e + ny, ny)
            block = rows_ref.at[froms[d], yy * nc + c]
            remote(block, block, xy_s.at[d, e], xy_r.at[d, e], at(z, x, ys[e], c)).wait_recv()
            for f in range(1, nc):
                go(block, block, xc_s.at[d, e, f], xc_r.at[d, e, f], at(z, x, y, cs[f]))
    for d in range(1, nz):
        block = w_ref.at[froms[d], x]
        remote(block, block, wz_s.at[d], wz_r.at[d], at(zs[d], x, y, c)).wait_recv()
        spread_w(block, froms[d], d)
    for d in range(nz):
        for e in range(1, nx):
            block = w_ref.at[froms[d], lax.rem(x - e + nx, nx)]
            remote(block, block, wx_s.at[d, e], wx_r.at[d, e], at(z, xs[e], y, c)).wait_recv()
        for e in range(ny):
            for f in range(1, nc):
                yy, cc = lax.rem(y - e + ny, ny), lax.rem(c - f + nc, nc)
                block = rows_ref.at[froms[d], yy * nc + cc]
                remote(block, block, xc_s.at[d, e, f], xc_r.at[d, e, f], at(z, x, y, cs[f])).wait_recv()
    for copy in sent:
        copy.wait_send()
    own_rows.wait()
    own_w.wait()


def gather(nz, nx, ny, nc, ident, rows, blocks):
    dma = pltpu.SemaphoreType.DMA
    return pl.pallas_call(
        functools.partial(gather_kernel, nz, nx, ny, nc),
        out_shape=(
            jax.ShapeDtypeStruct((nz, ny * nc) + rows.shape, rows.dtype),
            jax.ShapeDtypeStruct((nz, nx) + blocks.shape[1:], blocks.dtype),
        ),
        in_specs=[pl.BlockSpec(memory_space=pltpu.VMEM)] * 2,
        out_specs=[pl.BlockSpec(memory_space=pl.ANY)] * 2,
        scratch_shapes=[
            dma((2,)), dma((nz,)), dma((nz,)), dma((nz, ny)), dma((nz, ny)),
            dma((nz, ny, nc)), dma((nz, ny, nc)), dma((nz,)), dma((nz,)), dma((nz, nx)), dma((nz, nx)),
        ],
        compiler_params=pltpu.CompilerParams(collective_id=ident, has_side_effects=True),
        name="gather" + str(ident),
    )(rows, blocks)


def mix_kernel(nz, nx, nc, h_ref, o_ref, all_ref, w_ref, own_sem, hz_s, hz_r, wx_s, wx_r):
    z, x, y, c = place(nx, nc)
    at = lambda zz, xx: (zz * nx + xx, y * nc + c)
    zs = [lax.rem(z + d, nz) for d in range(nz)]
    xs = [lax.rem(x + d, nx) for d in range(nx)]
    greet([at(zs[d], x) for d in range(1, nz)] + [at(z, xs[d]) for d in range(1, nx)])
    wide, deep = h_ref.shape[1], o_ref.shape[1]
    h_at = lambda zz: all_ref.at[:, pl.ds(pl.multiple_of(zz * wide, wide), wide)]
    w_at = lambda xx: w_ref.at[:, pl.ds(pl.multiple_of(xx * deep, deep), deep)]
    copies = []
    for d in range(1, nz):
        copies.append(remote(h_ref, h_at(z), hz_s.at[d], hz_r.at[d], at(zs[d], x)))
    for e in range(1, nx):
        copies.append(remote(o_ref, w_at(x), wx_s.at[e], wx_r.at[e], at(z, xs[e])))
    copies.append(pltpu.make_async_copy(h_ref, h_at(z), own_sem.at[0]))
    copies.append(pltpu.make_async_copy(o_ref, w_at(x), own_sem.at[1]))
    for copy in copies:
        copy.start()
    for copy in copies:
        copy.wait()


def mix(nz, nx, nc, ident, hidden, out_weight):
    dma = pltpu.SemaphoreType.DMA
    return pl.pallas_call(
        functools.partial(mix_kernel, nz, nx, nc),
        out_shape=(
            jax.ShapeDtypeStruct((hidden.shape[0], hidden.shape[1] * nz), hidden.dtype),
            jax.ShapeDtypeStruct((out_weight.shape[0], out_weight.shape[1] * nx), out_weight.dtype),
        ),
        in_specs=[pl.BlockSpec(memory_space=pltpu.VMEM)] * 2,
        out_specs=[pl.BlockSpec(memory_space=pl.ANY)] * 2,
        scratch_shapes=[dma((2,)), dma((nz,)), dma((nz,)), dma((nx,)), dma((nx,))],
        compiler_params=pltpu.CompilerParams(collective_id=ident, has_side_effects=True),
        name="mix" + str(ident),
    )(hidden, out_weight)


def trade_kernel(nz, nx, nc, s_ref, r_ref, own_sem, z_s, z_r):
    z, x, y, c = place(nx, nc)
    at = lambda zz: (zz * nx + x, y * nc + c)
    zs = [lax.rem(z + d, nz) for d in range(nz)]
    greet([at(zs[d]) for d in range(1, nz)])
    copies = [
        remote(s_ref.at[zs[d]], r_ref.at[z], z_s.at[d], z_r.at[d], at(zs[d])) for d in range(1, nz)
    ]
    copies.append(pltpu.make_async_copy(s_ref.at[z], r_ref.at[z], own_sem.at[0]))
    for copy in copies:
        copy.start()
    for copy in copies:
        copy.wait()


def trade(nz, nx, nc, ident, sums):
    dma = pltpu.SemaphoreType.DMA
    return pl.pallas_call(
        functools.partial(trade_kernel, nz, nx, nc),
        out_shape=jax.ShapeDtypeStruct(sums.shape, sums.dtype),
        in_specs=[pl.BlockSpec(memory_space=pltpu.VMEM)],
        out_specs=pl.BlockSpec(memory_space=pltpu.VMEM),
        scratch_shapes=[dma((1,)), dma((nz,)), dma((nz,))],
        compiler_params=pltpu.CompilerParams(collective_id=ident, has_side_effects=True),
        name="trade" + str(ident),
    )(sums)


def per_device(
    nz, nx, ny, nc,
    tokens, query_weight, key_weight, value_weight, gate_weight, out_weight, sink_logits, out_gain,
):
    tp_count = ny * nc
    rows_here, width = tokens.shape
    block_rows = rows_here * tp_count
    heads_tp = query_weight.shape[2] // HEAD_DIM
    heads = heads_tp // nz
    cols = heads * HEAD_DIM
    kv = -(-heads // GROUP)
    kv_cols = kv * HEAD_DIM
    per_kv = heads // kv
    z = lax.div(lax.axis_index("sp"), nx)
    x = lax.rem(lax.axis_index("sp"), nx)
    head_start = lax.axis_index("tp") * heads_tp + z * heads

    offset = jnp.arange(WINDOW + block_rows) - WINDOW
    distance = jnp.arange(block_rows)[:, None] - offset[None, :]
    near = (distance >= 0) & (distance < WINDOW)
    start = (jnp.arange(nz) * nx + x) * block_rows
    visible = near[None] & ((start[:, None] + offset[None, :]) >= 0)[:, None, :]
    score_scale = HEAD_DIM ** (-0.5)
    turn = [(a * nx + b, a * nx + (b + 1) % nx) for a in range(nz) for b in range(nx)]

    def arranged(layer):
        parts = []
        for zz in range(nz):
            kv0 = (zz * heads // GROUP) * HEAD_DIM
            parts.append(
                jnp.concatenate(
                    [
                        query_weight[layer, :, zz * cols : (zz + 1) * cols],
                        gate_weight[layer, :, zz * cols : (zz + 1) * cols],
                        key_weight[layer, :, kv0 : kv0 + kv_cols],
                        value_weight[layer, :, kv0 : kv0 + kv_cols],
                    ],
                    axis=1,
                )
            )
        return jnp.stack(parts)

    current, result = tokens, None
    for layer in range(LAYERS):
        rows, joined = gather(nz, nx, ny, nc, 3 * layer, current, arranged(layer))
        rows = rows.reshape(nz * block_rows, width)
        joined = joined.reshape(width, joined.shape[-1])
        projected = jnp.dot(rows, joined, preferred_element_type=jnp.float32).astype(jnp.bfloat16)
        projected = projected.reshape(nz, block_rows, -1)
        own = projected[:, :, 2 * cols :]
        before = lax.ppermute(own[:, -WINDOW:], "sp", turn)
        later = jnp.concatenate([jnp.zeros_like(before[:1]), before[:-1]], axis=0)
        before = jnp.where(x == 0, later, before)
        nearby = jnp.concatenate([before, own], axis=1)
        queries = projected[:, :, :cols].reshape(nz, block_rows, kv, per_kv, HEAD_DIM)
        gate_part = projected[:, :, cols : 2 * cols]
        key_part = nearby[:, :, :kv_cols].reshape(nz, -1, kv, HEAD_DIM)
        value_part = nearby[:, :, kv_cols:].reshape(nz, -1, kv, HEAD_DIM)
        scores = (
            jnp.einsum("bqhgd,bkhd->bhgqk", queries, key_part, preferred_element_type=jnp.float32)
            * score_scale
        )
        scores = jnp.where(visible[:, None, None], scores, masked_score)
        sink = lax.dynamic_slice_in_dim(sink_logits[layer], head_start, heads, 0)
        sink = sink.reshape(1, kv, per_kv, 1, 1)
        highest = jnp.maximum(jnp.max(scores, axis=-1, keepdims=True), sink)
        exponent = jnp.exp(scores - highest)
        weights = (
            exponent / (jnp.sum(exponent, axis=-1, keepdims=True) + jnp.exp(sink - highest))
        ).astype(jnp.bfloat16)
        mixture = jnp.einsum(
            "bhgqk,bkhd->bqhgd", weights, value_part, preferred_element_type=jnp.float32
        ).reshape(nz, block_rows, cols)
        hidden = (mixture * jax.nn.silu(gate_part.astype(jnp.float32))).astype(jnp.bfloat16)
        hidden, out_cols = mix(
            nz, nx, nc, 3 * layer + 1, hidden.reshape(nz * block_rows, cols), out_weight[layer]
        )
        partial_value = jnp.dot(hidden, out_cols, preferred_element_type=jnp.float32)
        partial_value = partial_value.reshape(nz, tp_count, rows_here, -1)
        summed = lax.psum_scatter(partial_value, "tp", scatter_dimension=1, tiled=False)
        summed = trade(nz, nx, nc, 3 * layer + 2, summed)
        summed = jnp.swapaxes(summed, 0, 1).reshape(rows_here, width)
        factor = lax.rsqrt(jnp.mean(summed * summed, axis=-1, keepdims=True) + norm_epsilon)
        result = summed * factor * out_gain[layer]
        current = result.astype(jnp.bfloat16)
    return result


def solution(mesh):
    sp, tp = mesh.shape["sp"], mesh.shape["tp"]
    nc = 2 if tp % 2 == 0 else 1
    nx = next(n for n in range(1, sp + 1) if sp % n == 0 and n * n * nc >= sp)
    nz = sp // nx
    placed = (
        P(("sp", "tp"), None),
        P(None, "sp", "tp"),
        P(None, "sp", "tp"),
        P(None, "sp", "tp"),
        P(None, "sp", "tp"),
        P(None, "tp", "sp"),
        P(),
        P(),
    )
    return jax.shard_map(
        functools.partial(per_device, nz, nx, tp // nc, nc),
        mesh=mesh, in_specs=placed, out_specs=P(("sp", "tp"), None), check_vma=False,
    )
```

time: 1160 us -> 604 us (0.52)
  waiting for transfers between devices: 1070 us -> 90.3 us
  Pallas kernels: 0 us -> 424 us
  local copies, waits for them, and re-layouts: 8.66 us -> 20.7 us
    all_gather x6 -> x0, waiting for transfers between devices: 965 us -> none  [the longest x2 723 us: per_device(): lax.all_gather(joined, 'sp', axis=0, tiled=True)]
    pallas_call x0 -> x6, Pallas kernels: none -> 424 us  [the longest x2 263 us: gather(): pl.pallas_call(functools.partial(gather_kernel, nz, nx, ny, nc), out_shap...]
  transfers between devices with their start and end apart: 10 -> 4, of which waited for: 10 -> 4; matrix products, arithmetic and copies ran while one was open for 4% -> 1% of each run, Pallas kernels for 0% -> 0%
where the time goes in v1:
time: 604 us; the launch traced here: 603 us
  Pallas kernels  424 us (70%)
  waiting for transfers between devices  90.3 us (15%)
  matrix products  38.6 us (6%)
  local copies, waits for them, and re-layouts  20.7 us (3%)
  other arithmetic  15.1 us (2%)
  between operations  13.8 us (2%)
    pallas_call x2, Pallas kernels, gather(): pl.pallas_call(functools.partial(gather_kernel, nz, nx, ny, nc), out_shap...  263 us
    pallas_call x2, Pallas kernels, mix(): pl.pallas_call(functools.partial(mix_kernel, nz, nx, nc), out_shape=(jax....  104 us
    reduce_scatter x2, waiting for transfers between devices, per_device(): lax.psum_scatter(partial_value, 'tp', scatter_dimension=1, tiled=False)  86 us
    pallas_call x2, Pallas kernels, trade(): pl.pallas_call(functools.partial(trade_kernel, nz, nx, nc), out_shape=jax...  56.7 us
    dot_general x2, matrix products, per_device(): jnp.dot(rows, joined, preferred_element_type=jnp.float32)  21.4 us
  transfers between devices with their start and end apart: 4, of which 4 were waited for; matrix products, arithmetic and copies ran while one was open for 1% of the time, Pallas kernels for 0%

profile of v1, /device:TPU:9, one launch (start us, length us, event | category | flops | bytes accessed | tf_op | source)
XLA Modules:
  0.0 603.1 jit_solution(11917357834489808062)
XLA Ops:
  6.5 2.7 slice_bitcast_fusion.9
  9.3 1.1 slice_bitcast_fusion.8
  10.4 0.8 slice_bitcast_fusion.21
  11.2 0.8 slice_bitcast_fusion.20
  12.0 0.3 fusion.24
  12.2 1.9 pad_maximum_fusion.a_ref
  14.1 134.5 %gather0.1 = (bf16[4,4,64,4096]{3,2,1,0:T(8,128)(2,1)}, bf16[4,2,512,640]{3,2,1,0:T(8,128)(2,1)}) custom-call(bf16[64,4096]{1,0:T(8,128)(2,1)} %x_ref.1, bf16[4,512,640]{2,1,0:T(8,128)(2,1)} %pad_maximum_fusion.a_ref), custom_call_target="tpu_custom_call" | custom-call | tf_op jit(solution)/shard_map/gather0/pallas_call | solution.py:115
  148.6 10.7 %convolution_convert_fusion.1 = bf16[1024,640]{1,0:T(8,128)(2,1)S(1)} fusion(bf16[1024,4096]{1,0:T(8,128)(2,1)} %bitcast.201, bf16[4096,640]{1,0:T(8,128)(2,1)} %bitcast.203), kind=kOutput, calls=%fused_computation.17 | convolution fusion | flops 5369364480 | bytes 14942208 | tf_op jit(solution)/shard_map/dot_general | solution.py:245
  159.4 0.8 copy.38
  160.2 0.2 fusion.30
  160.4 0.1 add_compare_fusion
  160.5 1.5 slice_bitcast_fusion
  161.9 0.3 broadcast_and_fusion
  162.3 0.2 copy.20
  162.5 0.1 copy.39
  162.7 0.1 dynamic-slice_bitcast_fusion.1
  162.8 1.5 collective-permute-done
  164.3 1.2 fusion.2
  165.4 0.1 broadcast_maximum_fusion.1
  165.5 1.4 fusion
  166.9 0.1 exponential_add_fusion.1
  167.0 2.9 fusion.6
  169.9 1.6 copy.22
  171.5 1.1 fusion.19
  172.6 51.4 %mix1.1 = (bf16[1024,1024]{1,0:T(8,128)(2,1)}, bf16[1024,1024]{1,0:T(8,128)(2,1)}) custom-call(bf16[1024,256]{1,0:T(8,128)(2,1)} %bitcast.183, bf16[1024,512]{1,0:T(8,128)(2,1)} %get-tuple-element.22.o_ref), custom_call_target="tpu_custom_call" | custom-call | tf_op jit(solution)/shard_map/mix1/pallas_call | solution.py:156
  224.0 4.5 fusion.55
  228.5 2.3 copy.23
  231.0 0.8 copy-done.2
  231.7 0.1 copy-done.3
  231.8 0.1 copy-done.4
  231.9 0.1 copy-done.5
  232.0 0.1 copy-done.6
  232.1 0.1 copy-done.7
  232.1 0.1 copy-done.8
  232.2 0.1 copy-done.9
  232.5 0.3 fusion.20
  232.8 1.9 pad_maximum_fusion.1.a_ref
  234.7 40.6 %reduce-scatter.3.cloned.1.call-done = f32[4,1,64,1024]{3,2,0,1:T(8,128)} async-done(((f32[4,4,64,1024]{3,2,0,1:T(8,128)}), f32[4,1,64,1024]{3,2,0,1:T(8,128)}) %reduce-scatter.3.cloned.1.call-update) | async-done | bytes 1048592 | tf_op jit(solution)/shard_map/reduce_scatter | solution.py:277
  275.3 28.3 %trade2.1 = f32[4,64,1024]{2,1,0:T(8,128)} custom-call(f32[4,64,1024]{2,1,0:T(8,128)} %bitcast.194), custom_call_target="tpu_custom_call" | custom-call | tf_op jit(solution)/shard_map/trade2/pallas_call | solution.py:187
  303.6 1.4 fusion.17
  305.0 1.3 copy.42
  306.4 1.0 multiply_convert_fusion.x_ref
  307.3 128.8 %gather3.1 = (bf16[4,4,64,4096]{3,2,1,0:T(8,128)(2,1)}, bf16[4,2,512,640]{3,2,1,0:T(8,128)(2,1)}) custom-call(bf16[64,4096]{1,0:T(8,128)(2,1)} %multiply_convert_fusion.x_ref, bf16[4,512,640]{2,1,0:T(8,128)(2,1)} %pad_maximum_fusion.1.a_ref), custom_call_target="tpu_custom_call" | custom-call | tf_op jit(solution)/shard_map/gather3/pallas_call | solution.py:115
  436.2 10.6 %convolution_convert_fusion = bf16[1024,640]{1,0:T(8,128)(2,1)S(1)} fusion(bf16[1024,4096]{1,0:T(8,128)(2,1)} %bitcast.200, bf16[4096,640]{1,0:T(8,128)(2,1)} %bitcast.202), kind=kOutput, calls=%fused_computation.16 | convolution fusion | flops 5369364480 | bytes 14942208 | tf_op jit(solution)/shard_map/dot_general | solution.py:245
  446.8 0.1 copy.40
  446.9 0.5 collective-permute-start.1
  447.6 0.2 copy.27
  447.8 0.1 copy.41
  448.0 2.9 collective-permute-done.1
  450.9 1.2 fusion.3
  452.0 0.1 broadcast_maximum_fusion
  452.1 1.4 fusion.1
  453.5 0.1 exponential_add_fusion
  453.6 2.9 fusion.4
  456.5 1.6 copy.29
  458.1 1.1 fusion.18
  459.2 52.6 %mix4.1 = (bf16[1024,1024]{1,0:T(8,128)(2,1)}, bf16[1024,1024]{1,0:T(8,128)(2,1)}) custom-call(bf16[1024,256]{1,0:T(8,128)(2,1)} %bitcast.182, bf16[1024,512]{1,0:T(8,128)(2,1)} %get-tuple-element.21.o_ref), custom_call_target="tpu_custom_call" | custom-call | tf_op jit(solution)/shard_map/mix4/pallas_call | solution.py:156
  511.8 4.6 fusion.56
  516.3 2.3 copy.30
  518.6 45.4 %reduce-scatter.5.cloned.1.call-done = f32[4,1,64,1024]{3,2,0,1:T(8,128)} async-done(((f32[4,4,64,1024]{3,2,0,1:T(8,128)}), f32[4,1,64,1024]{3,2,0,1:T(8,128)}) %reduce-scatter.5.cloned.1.call-update) | async-done | bytes 1048592 | tf_op jit(solution)/shard_map/reduce_scatter | solution.py:277
  564.0 28.3 %trade5.1 = f32[4,64,1024]{2,1,0:T(8,128)} custom-call(f32[4,64,1024]{2,1,0:T(8,128)} %bitcast.195), custom_call_target="tpu_custom_call" | custom-call | tf_op jit(solution)/shard_map/trade5/pallas_call | solution.py:187
  592.3 1.4 fusion.16
  593.8 1.3 copy.43
  595.1 1.1 multiply_multiply_fusion
  (50 shorter events, 0.7 us)
Async XLA Ops:
  6.5 2.7 copy-start
  6.5 268.7 %reduce-scatter.3.cloned.1.call-start = ((), (), s32[]{:S(2)}) async-start(), calls=%async_computation.2 | async-start | bytes 5242880 | tf_op jit(solution)/shard_map/reduce_scatter | solution.py:277
  9.3 1.1 copy-start.10
  9.3 1.9 copy-start.11
  148.6 11.8 %copy-start.1 = (bf16[2,1024,512]{2,1,0:T(8,128)(2,1)S(1)}, bf16[2,1024,512]{2,1,0:T(8,128)(2,1)}, u32[]{:S(2)}) copy-start(bf16[2,1024,512]{2,1,0:T(8,128)(2,1)} %param.13) | copy-start | bytes 6291460
  159.4 2.8 copy-start.17
  160.2 4.0 collective-permute-start
  230.8 0.9 copy-start.2
  230.8 1.0 copy-start.3
  230.8 1.1 copy-start.4
  230.8 1.2 copy-start.5
  230.8 1.3 copy-start.6
  230.8 1.3 copy-start.7
  230.8 1.4 copy-start.8
  230.8 1.5 copy-start.9
  230.8 1.5 copy-start.12
  230.8 1.5 copy-start.13
  230.9 1.6 copy-start.14
  230.9 1.6 copy-start.15
  230.9 333.1 %reduce-scatter.5.cloned.1.call-start = ((), (), s32[]{:S(2)}) async-start(), calls=%async_computation.3 | async-start | bytes 5242880 | tf_op jit(solution)/shard_map/reduce_scatter | solution.py:277
  232.7 1.9 copy-start.16
  446.9 3.9 collective-permute-start.1
Sparse Core Ops, SparseCore 0:
  231.0 44.1 reduce-scatter.2
  518.8 45.2 reduce-scatter.4

commit v2 on v1

--- a/solution.py
+++ b/solution.py
@@ -33,6 +33,28 @@
     return pltpu.make_async_remote_copy(
         src_ref=src, dst_ref=dst, send_sem=send, recv_sem=recv, device_id=peer, device_id_type=MESH
     )
+
+
+def visits(z, nz, step, act):
+    if step == 0:
+        act(z, 0)
+        return
+    pl.when(z >= step)(lambda: act(z - step, 1))
+    pl.when(z + step < nz)(lambda: act(z + step, -1))
+
+
+def chain(z, nz, block, own, send, recv, peer):
+    def both(zz, way, use):
+        if way >= 0:
+            src = own if way == 0 else block(zz)
+            copy = remote(src, block(zz), send.at[0, zz], recv.at[zz], peer(z + 1))
+            pl.when(z + 1 < nz)(lambda: use(copy))
+        if way <= 0:
+            src = own if way == 0 else block(zz)
+            copy_down = remote(src, block(zz), send.at[1, zz], recv.at[zz], peer(z - 1))
+            pl.when(z >= 1)(lambda: use(copy_down))
+
+    return both
 
 
 def gather_kernel(
@@ -52,58 +74,88 @@
         + [at(z, x, y, cs[d]) for d in range(1, nc)]
     )
     sent = []
+    begin = lambda copy: copy.start()
+    end = lambda copy: copy.wait_send()
+    spot = lambda zz, yy, cc: rows_ref.at[zz, yy * nc + cc]
+    along = chain(z, nz, lambda zz: spot(zz, y, c), x_ref, xz_s, xz_r, lambda zz: at(zz, x, y, c))
+
+    def relay(zz, way, use):
+        src = x_ref if way == 0 else spot(zz, y, c)
+        for e in range(1, ny):
+            use(remote(src, spot(zz, y, c), xy_s.at[zz, e], xy_r.at[zz, e], at(z, x, ys[e], c)))
+        for f in range(1, nc):
+            use(remote(src, spot(zz, y, c), xc_s.at[zz, 0, f], xc_r.at[zz, 0, f], at(z, x, y, cs[f])))
+
+    def across(zz, use):
+        for e in range(1, ny):
+            block = spot(zz, lax.rem(y - e + ny, ny), c)
+            for f in range(1, nc):
+                use(remote(block, block, xc_s.at[zz, e, f], xc_r.at[zz, e, f], at(z, x, y, cs[f])))
+
+    def arrive(zz, way):
+        block = spot(zz, y, c)
+        remote(block, block, xz_s.at[0, zz], xz_r.at[zz], at(z, x, y, c)).wait_recv()
+        along(zz, way, begin)
+        relay(zz, way, begin)
+
+    def from_y(zz, way):
+        for e in range(1, ny):
+            block = spot(zz, lax.rem(y - e + ny, ny), c)
+            remote(block, block, xy_s.at[zz, e], xy_r.at[zz, e], at(z, x, ys[e], c)).wait_recv()
+        across(zz, begin)
+
+    def from_core(zz, way):
+        for e in range(ny):
+            for f in range(1, nc):
+                block = spot(zz, lax.rem(y - e + ny, ny), lax.rem(c - f + nc, nc))
+                remote(block, block, xc_s.at[zz, e, f], xc_r.at[zz, e, f], at(z, x, y, cs[f])).wait_recv()
+
+    def finish(zz, way):
+        along(zz, way, end)
+        relay(zz, way, end)
+        across(zz, end)
 
     def go(*args):
         copy = remote(*args)
         copy.start()
         sent.append(copy)
 
-    for d in range(1, nz):
-        go(x_ref, rows_ref.at[z, y * nc + c], xz_s.at[d], xz_r.at[d], at(zs[d], x, y, c))
-    for d in range(1, nz):
+    def send_w(d):
         go(a_ref.at[zs[d]], w_ref.at[z, x], wz_s.at[d], wz_r.at[d], at(zs[d], x, y, c))
-    own_rows = pltpu.make_async_copy(x_ref, rows_ref.at[z, y * nc + c], own_sem.at[0])
+
+    def spread_w(src, zz, d):
+        for e in range(1, nx):
+            go(src, w_ref.at[zz, x], wx_s.at[d, e], wx_r.at[d, e], at(z, xs[e], y, c))
+
+    froms = [lax.rem(z - d + nz, nz) for d in range(nz)]
+
+    def w_arrive(d):
+        block = w_ref.at[froms[d], x]
+        remote(block, block, wz_s.at[d], wz_r.at[d], at(zs[d], x, y, c)).wait_recv()
+        spread_w(block, froms[d], d)
+
+    along(z, 0, begin)
+    relay(z, 0, begin)
+    spread_w(a_ref.at[z], z, 0)
+    own_rows = pltpu.make_async_copy(x_ref, spot(z, y, c), own_sem.at[0])
     own_rows.start()
     own_w = pltpu.make_async_copy(a_ref.at[z], w_ref.at[z, x], own_sem.at[1])
     own_w.start()
-
-    def spread_rows(src, zz, d):
-        for e in range(1, ny):
-            go(src, rows_ref.at[zz, y * nc + c], xy_s.at[d, e], xy_r.at[d, e], at(z, x, ys[e], c))
-        for f in range(1, nc):
-            go(src, rows_ref.at[zz, y * nc + c], xc_s.at[d, 0, f], xc_r.at[d, 0, f], at(z, x, y, cs[f]))
-
-    def spread_w(src, zz, d):
+    send_w(1)
+    for step in range(1, nz):
+        visits(z, nz, step, arrive)
+        if step + 1 < nz:
+            send_w(step + 1)
+        w_arrive(step)
+    for step in range(nz):
+        visits(z, nz, step, from_y)
+    for step in range(nz):
+        visits(z, nz, step, from_core)
         for e in range(1, nx):
-            go(src, w_ref.at[zz, x], wx_s.at[d, e], wx_r.at[d, e], at(z, xs[e], y, c))
-
-    spread_w(a_ref.at[z], z, 0)
-    spread_rows(x_ref, z, 0)
-    froms = [lax.rem(z - d + nz, nz) for d in range(nz)]
-    for d in range(1, nz):
-        block = rows_ref.at[froms[d], y * nc + c]
-        remote(block, block, xz_s.at[d], xz_r.at[d], at(zs[d], x, y, c)).wait_recv()
-        spread_rows(block, froms[d], d)
-    for d in range(nz):
-        for e in range(1, ny):
-            yy = lax.rem(y - e + ny, ny)
-            block = rows_ref.at[froms[d], yy * nc + c]
-            remote(block, block, xy_s.at[d, e], xy_r.at[d, e], at(z, x, ys[e], c)).wait_recv()
-            for f in range(1, nc):
-                go(block, block, xc_s.at[d, e, f], xc_r.at[d, e, f], at(z, x, y, cs[f]))
-    for d in range(1, nz):
-        block = w_ref.at[froms[d], x]
-        remote(block, block, wz_s.at[d], wz_r.at[d], at(zs[d], x, y, c)).wait_recv()
-        spread_w(block, froms[d], d)
-    for d in range(nz):
-        for e in range(1, nx):
-            block = w_ref.at[froms[d], lax.rem(x - e + nx, nx)]
-            remote(block, block, wx_s.at[d, e], wx_r.at[d, e], at(z, xs[e], y, c)).wait_recv()
-        for e in range(ny):
-            for f in range(1, nc):
-                yy, cc = lax.rem(y - e + ny, ny), lax.rem(c - f + nc, nc)
-                block = rows_ref.at[froms[d], yy * nc + cc]
-                remote(block, block, xc_s.at[d, e, f], xc_r.at[d, e, f], at(z, x, y, cs[f])).wait_recv()
+            block = w_ref.at[froms[step], lax.rem(x - e + nx, nx)]
+            remote(block, block, wx_s.at[step, e], wx_r.at[step, e], at(z, xs[e], y, c)).wait_recv()
+    for step in range(nz):
+        visits(z, nz, step, finish)
     for copy in sent:
         copy.wait_send()
     own_rows.wait()
@@ -121,7 +173,7 @@
         in_specs=[pl.BlockSpec(memory_space=pltpu.VMEM)] * 2,
         out_specs=[pl.BlockSpec(memory_space=pl.ANY)] * 2,
         scratch_shapes=[
-            dma((2,)), dma((nz,)), dma((nz,)), dma((nz, ny)), dma((nz, ny)),
+            dma((2,)), dma((2, nz)), dma((nz,)), dma((nz, ny)), dma((nz, ny)),
             dma((nz, ny, nc)), dma((nz, ny, nc)), dma((nz,)), dma((nz,)), dma((nz, nx)), dma((nz, nx)),
         ],
         compiler_params=pltpu.CompilerParams(collective_id=ident, has_side_effects=True),
@@ -138,17 +190,26 @@
     wide, deep = h_ref.shape[1], o_ref.shape[1]
     h_at = lambda zz: all_ref.at[:, pl.ds(pl.multiple_of(zz * wide, wide), wide)]
     w_at = lambda xx: w_ref.at[:, pl.ds(pl.multiple_of(xx * deep, deep), deep)]
+    along = chain(z, nz, h_at, h_ref, hz_s, hz_r, lambda zz: at(zz, x))
     copies = []
-    for d in range(1, nz):
-        copies.append(remote(h_ref, h_at(z), hz_s.at[d], hz_r.at[d], at(zs[d], x)))
     for e in range(1, nx):
         copies.append(remote(o_ref, w_at(x), wx_s.at[e], wx_r.at[e], at(z, xs[e])))
     copies.append(pltpu.make_async_copy(h_ref, h_at(z), own_sem.at[0]))
     copies.append(pltpu.make_async_copy(o_ref, w_at(x), own_sem.at[1]))
+    along(z, 0, lambda copy: copy.start())
     for copy in copies:
         copy.start()
+
+    def arrive(zz, way):
+        remote(h_at(zz), h_at(zz), hz_s.at[0, zz], hz_r.at[zz], at(z, x)).wait_recv()
+        along(zz, way, lambda copy: copy.start())
+
+    for step in range(1, nz):
+        visits(z, nz, step, arrive)
     for copy in copies:
         copy.wait()
+    for step in range(nz):
+        visits(z, nz, step, lambda zz, way: along(zz, way, lambda copy: copy.wait_send()))
 
 
 def mix(nz, nx, nc, ident, hidden, out_weight):
@@ -161,38 +222,88 @@
         ),
         in_specs=[pl.BlockSpec(memory_space=pltpu.VMEM)] * 2,
         out_specs=[pl.BlockSpec(memory_space=pl.ANY)] * 2,
-        scratch_shapes=[dma((2,)), dma((nz,)), dma((nz,)), dma((nx,)), dma((nx,))],
+        scratch_shapes=[dma((2,)), dma((2, nz)), dma((nz,)), dma((nx,)), dma((nx,))],
         compiler_params=pltpu.CompilerParams(collective_id=ident, has_side_effects=True),
         name="mix" + str(ident),
     )(hidden, out_weight)
 
 
-def trade_kernel(nz, nx, nc, s_ref, r_ref, own_sem, z_s, z_r):
+def settle_kernel(
+    nz, nx, ny, nc, p_ref, r_ref, from_c, from_y, half, whole,
+    c_s, c_r, y_s, y_r, z_s, z_r,
+):
     z, x, y, c = place(nx, nc)
-    at = lambda zz: (zz * nx + x, y * nc + c)
+    at = lambda zz, yy, cc: (zz * nx + x, yy * nc + cc)
     zs = [lax.rem(z + d, nz) for d in range(nz)]
-    greet([at(zs[d]) for d in range(1, nz)])
-    copies = [
-        remote(s_ref.at[zs[d]], r_ref.at[z], z_s.at[d], z_r.at[d], at(zs[d])) for d in range(1, nz)
-    ]
-    copies.append(pltpu.make_async_copy(s_ref.at[z], r_ref.at[z], own_sem.at[0]))
-    for copy in copies:
+    ys = [lax.rem(y + d, ny) for d in range(ny)]
+    cs = [lax.rem(c + d, nc) for d in range(nc)]
+    greet(
+        [at(zs[d], y, c) for d in range(1, nz)]
+        + [at(z, ys[d], c) for d in range(1, ny)]
+        + [at(z, y, cs[d]) for d in range(1, nc)]
+    )
+    order = list(range(1, nz)) + [0]
+    far = list(range(1, ny)) + [0]
+    sent = []
+
+    def go(*args):
+        copy = remote(*args)
         copy.start()
-    for copy in copies:
-        copy.wait()
-
-
-def trade(nz, nx, nc, ident, sums):
+        sent.append(copy)
+
+    for d in order:
+        for e in far:
+            for f in range(1, nc):
+                go(
+                    p_ref.at[zs[d], ys[e] * nc + cs[f]], from_c.at[d, e, f],
+                    c_s.at[d, e, f], c_r.at[d, e, f], at(z, y, cs[f]),
+                )
+    for d in order:
+        for e in far:
+            total = p_ref[zs[d], ys[e] * nc + c]
+            for f in range(1, nc):
+                part = from_c.at[d, e, f]
+                remote(part, part, c_s.at[d, e, f], c_r.at[d, e, f], at(z, y, cs[f])).wait_recv()
+                total = total + part[...]
+            half[d, e] = total
+            if e > 0:
+                go(half.at[d, e], from_y.at[d, e], y_s.at[d, e], y_r.at[d, e], at(z, ys[e], c))
+    for d in order:
+        total = half[d, 0]
+        for e in range(1, ny):
+            part = from_y.at[d, e]
+            remote(part, part, y_s.at[d, e], y_r.at[d, e], at(z, ys[e], c)).wait_recv()
+            total = total + part[...]
+        if d > 0:
+            whole[d] = total
+            go(whole.at[d], r_ref.at[z], z_s.at[d], z_r.at[d], at(zs[d], y, c))
+        else:
+            r_ref[z] = total
+    for d in range(1, nz):
+        block = r_ref.at[lax.rem(z - d + nz, nz)]
+        remote(block, block, z_s.at[d], z_r.at[d], at(zs[d], y, c)).wait_recv()
+    for copy in sent:
+        copy.wait_send()
+
+
+def settle(nz, nx, ny, nc, ident, partial):
     dma = pltpu.SemaphoreType.DMA
+    block = partial.shape[2:]
     return pl.pallas_call(
-        functools.partial(trade_kernel, nz, nx, nc),
-        out_shape=jax.ShapeDtypeStruct(sums.shape, sums.dtype),
+        functools.partial(settle_kernel, nz, nx, ny, nc),
+        out_shape=jax.ShapeDtypeStruct((nz,) + block, partial.dtype),
         in_specs=[pl.BlockSpec(memory_space=pltpu.VMEM)],
         out_specs=pl.BlockSpec(memory_space=pltpu.VMEM),
-        scratch_shapes=[dma((1,)), dma((nz,)), dma((nz,))],
+        scratch_shapes=[
+            pltpu.VMEM((nz, ny, nc) + block, partial.dtype),
+            pltpu.VMEM((nz, ny) + block, partial.dtype),
+            pltpu.VMEM((nz, ny) + block, partial.dtype),
+            pltpu.VMEM((nz,) + block, partial.dtype),
+            dma((nz, ny, nc)), dma((nz, ny, nc)), dma((nz, ny)), dma((nz, ny)), dma((nz,)), dma((nz,)),
+        ],
         compiler_params=pltpu.CompilerParams(collective_id=ident, has_side_effects=True),
-        name="trade" + str(ident),
-    )(sums)
+        name="settle" + str(ident),
+    )(partial)
 
 
 def per_device(
@@ -274,8 +385,7 @@
         )
         partial_value = jnp.dot(hidden, out_cols, preferred_element_type=jnp.float32)
         partial_value = partial_value.reshape(nz, tp_count, rows_here, -1)
-        summed = lax.psum_scatter(partial_value, "tp", scatter_dimension=1, tiled=False)
-        summed = trade(nz, nx, nc, 3 * layer + 2, summed)
+        summed = settle(nz, nx, ny, nc, 3 * layer + 2, partial_value)
         summed = jnp.swapaxes(summed, 0, 1).reshape(rows_here, width)
         factor = lax.rsqrt(jnp.mean(summed * summed, axis=-1, keepdims=True) + norm_epsilon)
         result = summed * factor * out_gain[layer]

time: 604 us -> 462 us (0.76)
  waiting for transfers between devices: 90.3 us -> 2.32 us
  Pallas kernels: 424 us -> 383 us
  between operations: 13.8 us -> 0.32 us
    reduce_scatter x2 -> x0, waiting for transfers between devices: 86 us -> none  [per_device(): lax.psum_scatter(partial_value, 'tp', scatter_dimension=1, tiled=False)]
    pallas_call x2, Pallas kernels: 263 us -> 195 us  [gather(): pl.pallas_call(functools.partial(gather_kernel, nz, nx, ny, nc), out_shap...]
    pallas_call x2, Pallas kernels: 56.7 us -> 86.5 us  [settle(): pl.pallas_call(functools.partial(settle_kernel, nz, nx, ny, nc), out_shap...]
  transfers between devices with their start and end apart: 4 -> 2, of which waited for: 4 -> 1; matrix products, arithmetic and copies ran while one was open for 1% -> 1% of each run, Pallas kernels for 0% -> 0%
where the time goes in v2:
time: 462 us
  Pallas kernels  383 us (83%)
  matrix products  42.5 us (9%)
  other arithmetic  16.5 us (4%)
  local copies, waits for them, and re-layouts  16 us (3%)
    pallas_call x2, Pallas kernels, gather(): pl.pallas_call(functools.partial(gather_kernel, nz, nx, ny, nc), out_shap...  195 us
    pallas_call x2, Pallas kernels, mix(): pl.pallas_call(functools.partial(mix_kernel, nz, nx, nc), out_shape=(jax....  101 us
    pallas_call x2, Pallas kernels, settle(): pl.pallas_call(functools.partial(settle_kernel, nz, nx, ny, nc), out_shap...  86.5 us
    dot_general x2, matrix products, per_device(): jnp.dot(rows, joined, preferred_element_type=jnp.float32)  21.4 us
    dot_general x2, matrix products, per_device(): jnp.dot(hidden, out_cols, preferred_element_type=jnp.float32)  13 us
  transfers between devices with their start and end apart: 2, of which 1 were waited for; matrix products, arithmetic and copies ran while one was open for 1% of the time, Pallas kernels for 0%

profile of v2, /device:TPU:9, one launch (start us, length us, event | category | flops | bytes accessed | tf_op | source)
XLA Modules:
  0.0 461.6 jit_solution(3895036663530423861)
XLA Ops:
  0.0 1.8 slice_bitcast_fusion.9
  1.8 0.4 copy-done
  2.3 1.0 slice_bitcast_fusion.8
  3.3 0.0 copy-done.4
  3.3 0.8 slice_bitcast_fusion.21
  4.1 0.0 copy-done.5
  4.1 0.8 slice_bitcast_fusion.20
  4.8 0.3 fusion.24
  5.1 1.9 pad_maximum_fusion.a_ref
  7.0 97.3 %gather0.1 = (bf16[4,4,64,4096]{3,2,1,0:T(8,128)(2,1)}, bf16[4,2,512,640]{3,2,1,0:T(8,128)(2,1)}) custom-call(bf16[64,4096]{1,0:T(8,128)(2,1)} %x_ref.1, bf16[4,512,640]{2,1,0:T(8,128)(2,1)} %pad_maximum_fusion.a_ref), custom_call_target="tpu_custom_call" | custom-call | tf_op jit(solution)/shard_map/gather0/pallas_call | solution.py:167
  104.3 0.0 copy-start.1
  104.3 10.7 %convolution_convert_fusion.1 = bf16[1024,640]{1,0:T(8,128)(2,1)S(1)} fusion(bf16[1024,4096]{1,0:T(8,128)(2,1)} %bitcast.197, bf16[4096,640]{1,0:T(8,128)(2,1)} %bitcast.199), kind=kOutput, calls=%fused_computation.17 | convolution fusion | flops 5369364480 | bytes 14942208 | tf_op jit(solution)/shard_map/dot_general | solution.py:356
  115.0 0.0 copy-start.2
  115.0 0.0 copy-start.6
  115.1 1.1 copy-done.2
  116.1 0.8 copy.36
  116.9 0.2 collective-permute-start
  117.2 0.2 fusion.30
  117.3 0.1 add_compare_fusion
  117.4 0.0 copy-done.1
  117.4 1.5 slice_bitcast_fusion
  118.9 0.3 broadcast_and_fusion
  119.2 1.7 fusion.20
  120.9 0.0 copy-start.7
  120.9 1.9 pad_maximum_fusion.1.a_ref
  122.9 0.2 copy.20
  123.1 0.1 copy.37
  123.2 0.1 dynamic-slice_bitcast_fusion.1
  123.3 0.0 collective-permute-done
  123.3 0.9 slice.187
  124.2 1.2 fusion.2
  125.4 0.1 broadcast_maximum_fusion.1
  125.5 1.4 fusion
  126.9 0.1 exponential_add_fusion.1
  127.0 2.9 fusion.6
  129.9 1.6 copy.22
  131.4 1.1 fusion.19
  132.5 50.8 %mix1.1 = (bf16[1024,1024]{1,0:T(8,128)(2,1)}, bf16[1024,1024]{1,0:T(8,128)(2,1)}) custom-call(bf16[1024,256]{1,0:T(8,128)(2,1)} %bitcast.181, bf16[1024,512]{1,0:T(8,128)(2,1)} %get-tuple-element.22.o_ref), custom_call_target="tpu_custom_call" | custom-call | tf_op jit(solution)/shard_map/mix1/pallas_call | solution.py:217
  183.4 6.5 %fusion.55 = f32[1024,1024]{1,0:T(8,128)} fusion(bf16[1024,1024]{1,0:T(8,128)(2,1)} %get-tuple-element.15, bf16[1024,1024]{1,0:T(8,128)(2,1)} %get-tuple-element.16), kind=kOutput, calls=%fused_computation.132 | convolution fusion | flops 2147483648 | bytes 8388608 | tf_op jit(solution)/shard_map/dot_general | solution.py:386
  189.9 43.6 %settle2.1 = f32[4,64,1024]{2,1,0:T(8,128)} custom-call(f32[4,4,64,1024]{3,2,1,0:T(8,128)} %bitcast.176), custom_call_target="tpu_custom_call" | custom-call | tf_op jit(solution)/shard_map/settle2/pallas_call | solution.py:292
  233.4 1.4 fusion.17
  234.8 1.3 copy.40
  236.2 1.0 multiply_convert_fusion.x_ref
  237.2 97.7 %gather3.1 = (bf16[4,4,64,4096]{3,2,1,0:T(8,128)(2,1)}, bf16[4,2,512,640]{3,2,1,0:T(8,128)(2,1)}) custom-call(bf16[64,4096]{1,0:T(8,128)(2,1)} %multiply_convert_fusion.x_ref, bf16[4,512,640]{2,1,0:T(8,128)(2,1)} %pad_maximum_fusion.1.a_ref), custom_call_target="tpu_custom_call" | custom-call | tf_op jit(solution)/shard_map/gather3/pallas_call | solution.py:167
  334.9 10.6 %convolution_convert_fusion = bf16[1024,640]{1,0:T(8,128)(2,1)S(1)} fusion(bf16[1024,4096]{1,0:T(8,128)(2,1)} %bitcast.196, bf16[4096,640]{1,0:T(8,128)(2,1)} %bitcast.198), kind=kOutput, calls=%fused_computation.16 | convolution fusion | flops 5369364480 | bytes 14942208 | tf_op jit(solution)/shard_map/dot_general | solution.py:356
  345.6 0.1 copy.38
  345.7 1.0 collective-permute-start.1
  346.7 0.1 dynamic-slice_bitcast_fusion
  346.9 0.2 copy.26
  347.1 0.1 copy.39
  347.3 2.3 collective-permute-done.1
  349.6 1.2 fusion.3
  350.8 0.1 broadcast_maximum_fusion
  350.9 1.4 fusion.1
  352.3 0.1 exponential_add_fusion
  352.4 2.9 fusion.4
  355.3 1.6 copy.28
  356.8 1.1 fusion.18
  357.9 50.4 %mix4.1 = (bf16[1024,1024]{1,0:T(8,128)(2,1)}, bf16[1024,1024]{1,0:T(8,128)(2,1)}) custom-call(bf16[1024,256]{1,0:T(8,128)(2,1)} %bitcast.180, bf16[1024,512]{1,0:T(8,128)(2,1)} %get-tuple-element.21.o_ref), custom_call_target="tpu_custom_call" | custom-call | tf_op jit(solution)/shard_map/mix4/pallas_call | solution.py:217
  408.3 6.5 %fusion.56 = f32[1024,1024]{1,0:T(8,128)} fusion(bf16[1024,1024]{1,0:T(8,128)(2,1)} %get-tuple-element.19, bf16[1024,1024]{1,0:T(8,128)(2,1)} %get-tuple-element.20), kind=kOutput, calls=%fused_computation.133 | convolution fusion | flops 2147483648 | bytes 8388608 | tf_op jit(solution)/shard_map/dot_general | solution.py:386
  414.8 42.9 %settle5.1 = f32[4,64,1024]{2,1,0:T(8,128)} custom-call(f32[4,4,64,1024]{3,2,1,0:T(8,128)} %bitcast.177), custom_call_target="tpu_custom_call" | custom-call | tf_op jit(solution)/shard_map/settle5/pallas_call | solution.py:292
  457.7 1.4 fusion.16
  459.1 1.3 copy.41
  460.5 1.1 multiply_multiply_fusion
  (22 shorter events, 0.3 us)
Async XLA Ops:
  0.0 2.3 copy-start
  2.3 1.0 copy-start.4
  2.3 1.8 copy-start.5
  104.3 13.1 %copy-start.1 = (bf16[2,1024,512]{2,1,0:T(8,128)(2,1)S(1)}, bf16[2,1024,512]{2,1,0:T(8,128)(2,1)}, u32[]{:S(2)}) copy-start(bf16[2,1024,512]{2,1,0:T(8,128)(2,1)} %param.13) | copy-start | bytes 6291460
  115.0 1.1 copy-start.2
  115.0 3.8 copy-start.6
  116.9 6.4 %collective-permute-start = (bf16[4,128,128]{1,2,0:T(8,128)(2,1)}, bf16[4,128,128]{1,2,0:T(8,128)(2,1)}, u32[]{:S(2)}, u32[]{:S(2)}) collective-permute-start(bf16[4,128,128]{1,2,0:T(8,128)(2,1)} %copy.36), channel_id=1, source_target_pairs={{0,4},{4,0},{8,12},{12,8},{16,20},{20,16},{24,28},{28,24},{1,5},{5... | collective-permute-start | bytes 393224 | tf_op jit(solution)/shard_map/ppermute | solution.py:359
  120.9 1.9 copy-start.7
  120.9 1.9 copy-start.3
  345.7 3.9 collective-permute-start.1

commit v3 on v2

--- a/solution.py
+++ b/solution.py
@@ -58,7 +58,7 @@
 
 
 def gather_kernel(
-    nz, nx, ny, nc, x_ref, a_ref, rows_ref, w_ref,
+    nz, nx, ny, nc, layer, x_ref, q_ref, g_ref, a_ref, rows_ref, w_ref,
     own_sem, xz_s, xz_r, xy_s, xy_r, xc_s, xc_r, wz_s, wz_r, wx_s, wx_r,
 ):
     z, x, y, c = place(nx, nc)
@@ -115,17 +115,31 @@
         relay(zz, way, end)
         across(zz, end)
 
-    def go(*args):
-        copy = remote(*args)
-        copy.start()
-        sent.append(copy)
+    cols = q_ref.shape[2] // nz
+
+    def pieces(zz):
+        here = pl.ds(pl.multiple_of(zz * cols, cols), cols)
+        rest = pl.ds(2 * cols, a_ref.shape[2])
+        return (
+            (q_ref.at[layer, :, here], w_ref.at[z, x, :, pl.ds(0, cols)]),
+            (g_ref.at[layer, :, here], w_ref.at[z, x, :, pl.ds(cols, cols)]),
+            (a_ref.at[zz], w_ref.at[z, x, :, rest]),
+        )
+
+    def send_own(zz, send, recv, peer):
+        for src, dst in pieces(zz):
+            remote(src, dst, send, recv, peer).start()
+        block = w_ref.at[z, x]
+        sent.append(remote(block, block, send, recv, peer))
 
     def send_w(d):
-        go(a_ref.at[zs[d]], w_ref.at[z, x], wz_s.at[d], wz_r.at[d], at(zs[d], x, y, c))
+        send_own(zs[d], wz_s.at[d], wz_r.at[d], at(zs[d], x, y, c))
 
     def spread_w(src, zz, d):
         for e in range(1, nx):
-            go(src, w_ref.at[zz, x], wx_s.at[d, e], wx_r.at[d, e], at(z, xs[e], y, c))
+            copy = remote(src, w_ref.at[zz, x], wx_s.at[d, e], wx_r.at[d, e], at(z, xs[e], y, c))
+            copy.start()
+            sent.append(copy)
 
     froms = [lax.rem(z - d + nz, nz) for d in range(nz)]
 
@@ -136,11 +150,12 @@
 
     along(z, 0, begin)
     relay(z, 0, begin)
-    spread_w(a_ref.at[z], z, 0)
+    for e in range(1, nx):
+        send_own(z, wx_s.at[0, e], wx_r.at[0, e], at(z, xs[e], y, c))
     own_rows = pltpu.make_async_copy(x_ref, spot(z, y, c), own_sem.at[0])
     own_rows.start()
-    own_w = pltpu.make_async_copy(a_ref.at[z], w_ref.at[z, x], own_sem.at[1])
-    own_w.start()
+    for src, dst in pieces(z):
+        pltpu.make_async_copy(src, dst, own_sem.at[1]).start()
     send_w(1)
     for step in range(1, nz):
         visits(z, nz, step, arrive)
@@ -159,18 +174,24 @@
     for copy in sent:
         copy.wait_send()
     own_rows.wait()
-    own_w.wait()
-
-
-def gather(nz, nx, ny, nc, ident, rows, blocks):
+    pltpu.make_async_copy(w_ref.at[z, x], w_ref.at[z, x], own_sem.at[1]).wait()
+
+
+def gather(nz, nx, ny, nc, layer, ident, rows, query, gate, blocks):
     dma = pltpu.SemaphoreType.DMA
+    block = (blocks.shape[1], 2 * query.shape[2] // nz + blocks.shape[2])
     return pl.pallas_call(
-        functools.partial(gather_kernel, nz, nx, ny, nc),
+        functools.partial(gather_kernel, nz, nx, ny, nc, layer),
         out_shape=(
             jax.ShapeDtypeStruct((nz, ny * nc) + rows.shape, rows.dtype),
-            jax.ShapeDtypeStruct((nz, nx) + blocks.shape[1:], blocks.dtype),
+            jax.ShapeDtypeStruct((nz, nx) + block, blocks.dtype),
         ),
-        in_specs=[pl.BlockSpec(memory_space=pltpu.VMEM)] * 2,
+        in_specs=[
+            pl.BlockSpec(memory_space=pltpu.VMEM),
+            pl.BlockSpec(memory_space=pl.ANY),
+            pl.BlockSpec(memory_space=pl.ANY),
+            pl.BlockSpec(memory_space=pltpu.VMEM),
+        ],
         out_specs=[pl.BlockSpec(memory_space=pl.ANY)] * 2,
         scratch_shapes=[
             dma((2,)), dma((2, nz)), dma((nz,)), dma((nz, ny)), dma((nz, ny)),
@@ -178,7 +199,7 @@
         ],
         compiler_params=pltpu.CompilerParams(collective_id=ident, has_side_effects=True),
         name="gather" + str(ident),
-    )(rows, blocks)
+    )(rows, query, gate, blocks)
 
 
 def mix_kernel(nz, nx, nc, h_ref, o_ref, all_ref, w_ref, own_sem, hz_s, hz_r, wx_s, wx_r):
@@ -229,7 +250,7 @@
 
 
 def settle_kernel(
-    nz, nx, ny, nc, p_ref, r_ref, from_c, from_y, half, whole,
+    nz, nx, ny, nc, p_ref, r_ref, from_c, from_y, out_y, half, whole,
     c_s, c_r, y_s, y_r, z_s, z_r,
 ):
     z, x, y, c = place(nx, nc)
@@ -265,20 +286,22 @@
                 part = from_c.at[d, e, f]
                 remote(part, part, c_s.at[d, e, f], c_r.at[d, e, f], at(z, y, cs[f])).wait_recv()
                 total = total + part[...]
-            half[d, e] = total
-            if e > 0:
-                go(half.at[d, e], from_y.at[d, e], y_s.at[d, e], y_r.at[d, e], at(z, ys[e], c))
+            if e == 0:
+                half[d] = total
+            else:
+                out_y[d, e] = total.astype(out_y.dtype)
+                go(out_y.at[d, e], from_y.at[d, e], y_s.at[d, e], y_r.at[d, e], at(z, ys[e], c))
     for d in order:
-        total = half[d, 0]
+        total = half[d]
         for e in range(1, ny):
             part = from_y.at[d, e]
             remote(part, part, y_s.at[d, e], y_r.at[d, e], at(z, ys[e], c)).wait_recv()
-            total = total + part[...]
+            total = total + part[...].astype(jnp.float32)
         if d > 0:
-            whole[d] = total
+            whole[d] = total.astype(whole.dtype)
             go(whole.at[d], r_ref.at[z], z_s.at[d], z_r.at[d], at(zs[d], y, c))
         else:
-            r_ref[z] = total
+            r_ref[z] = total.astype(r_ref.dtype)
     for d in range(1, nz):
         block = r_ref.at[lax.rem(z - d + nz, nz)]
         remote(block, block, z_s.at[d], z_r.at[d], at(zs[d], y, c)).wait_recv()
@@ -291,14 +314,15 @@
     block = partial.shape[2:]
     return pl.pallas_call(
         functools.partial(settle_kernel, nz, nx, ny, nc),
-        out_shape=jax.ShapeDtypeStruct((nz,) + block, partial.dtype),
+        out_shape=jax.ShapeDtypeStruct((nz,) + block, jnp.bfloat16),
         in_specs=[pl.BlockSpec(memory_space=pltpu.VMEM)],
         out_specs=pl.BlockSpec(memory_space=pltpu.VMEM),
         scratch_shapes=[
             pltpu.VMEM((nz, ny, nc) + block, partial.dtype),
-            pltpu.VMEM((nz, ny) + block, partial.dtype),
-            pltpu.VMEM((nz, ny) + block, partial.dtype),
+            pltpu.VMEM((nz, ny) + block, jnp.bfloat16),
+            pltpu.VMEM((nz, ny) + block, jnp.bfloat16),
             pltpu.VMEM((nz,) + block, partial.dtype),
+            pltpu.VMEM((nz,) + block, jnp.bfloat16),
             dma((nz, ny, nc)), dma((nz, ny, nc)), dma((nz, ny)), dma((nz, ny)), dma((nz,)), dma((nz,)),
         ],
         compiler_params=pltpu.CompilerParams(collective_id=ident, has_side_effects=True),
@@ -338,8 +362,6 @@
             parts.append(
                 jnp.concatenate(
                     [
-                        query_weight[layer, :, zz * cols : (zz + 1) * cols],
-                        gate_weight[layer, :, zz * cols : (zz + 1) * cols],
                         key_weight[layer, :, kv0 : kv0 + kv_cols],
                         value_weight[layer, :, kv0 : kv0 + kv_cols],
                     ],
@@ -350,7 +372,9 @@
 
     current, result = tokens, None
     for layer in range(LAYERS):
-        rows, joined = gather(nz, nx, ny, nc, 3 * layer, current, arranged(layer))
+        rows, joined = gather(
+            nz, nx, ny, nc, layer, 3 * layer, current, query_weight, gate_weight, arranged(layer)
+        )
         rows = rows.reshape(nz * block_rows, width)
         joined = joined.reshape(width, joined.shape[-1])
         projected = jnp.dot(rows, joined, preferred_element_type=jnp.float32).astype(jnp.bfloat16)
@@ -386,7 +410,7 @@
         partial_value = jnp.dot(hidden, out_cols, preferred_element_type=jnp.float32)
         partial_value = partial_value.reshape(nz, tp_count, rows_here, -1)
         summed = settle(nz, nx, ny, nc, 3 * layer + 2, partial_value)
-        summed = jnp.swapaxes(summed, 0, 1).reshape(rows_here, width)
+        summed = jnp.swapaxes(summed, 0, 1).reshape(rows_here, width).astype(jnp.float32)
         factor = lax.rsqrt(jnp.mean(summed * summed, axis=-1, keepdims=True) + norm_epsilon)
         result = summed * factor * out_gain[layer]
         current = result.astype(jnp.bfloat16)

time: 462 us -> 430 us (0.931)
  Pallas kernels: 383 us -> 352 us
    pallas_call x2, Pallas kernels: 86.5 us -> 57 us  [settle(): pl.pallas_call(functools.partial(settle_kernel, nz, nx, ny, nc), out_shap...]
  transfers between devices with their start and end apart: 2 -> 2, of which waited for: 1 -> 1; matrix products, arithmetic and copies ran while one was open for 1% -> 2% of each run, Pallas kernels for 0% -> 0%
where the time goes in v3:
time: 430 us; the launch traced here: 429 us
  Pallas kernels  352 us (82%)
  matrix products  42.5 us (10%)
  other arithmetic  18 us (4%)
  local copies, waits for them, and re-layouts  12.7 us (3%)
    pallas_call x2, Pallas kernels, gather(): pl.pallas_call(functools.partial(gather_kernel, nz, nx, ny, nc, layer), o...  194 us
    pallas_call x2, Pallas kernels, mix(): pl.pallas_call(functools.partial(mix_kernel, nz, nx, nc), out_shape=(jax....  101 us
    pallas_call x2, Pallas kernels, settle(): pl.pallas_call(functools.partial(settle_kernel, nz, nx, ny, nc), out_shap...  57 us
    dot_general x2, matrix products, per_device(): jnp.dot(rows, joined, preferred_element_type=jnp.float32)  21.4 us
    dot_general x2, matrix products, per_device(): jnp.dot(hidden, out_cols, preferred_element_type=jnp.float32)  13 us
  transfers between devices with their start and end apart: 2, of which 1 were waited for; matrix products, arithmetic and copies ran while one was open for 2% of the time, Pallas kernels for 0%

profile of v3, /device:TPU:9, one launch (start us, length us, event | category | flops | bytes accessed | tf_op | source)
XLA Modules:
  0.0 429.0 jit_solution(11236174222851610474)
XLA Ops:
  0.0 1.9 slice_bitcast_fusion.5
  1.9 1.9 slice_bitcast_fusion.4
  3.8 0.1 maximum_bitcast_fusion
  3.9 0.8 pad_maximum_fusion.a_ref
  4.8 96.8 %gather0.1 = (bf16[4,4,64,4096]{3,2,1,0:T(8,128)(2,1)}, bf16[4,2,512,640]{3,2,1,0:T(8,128)(2,1)}) custom-call(bf16[64,4096]{1,0:T(8,128)(2,1)} %x_ref.1, bf16[2,512,1024]{2,1,0:T(8,128)(2,1)} %q_ref.3, bf16[2,512,1024]{2,1,0:T(8,128)(2,1)} %g_ref.3, bf16[4,512,128]{2,1,0:T(8,128)(2,1)} %pad_maximum_fusion.a_ref), custom_call_target="tpu_custom_call" | custom-call | tf_op jit(solution)/shard_map/gather0/pallas_call | solution.py:183
  101.5 0.0 copy-start.1
  101.6 0.0 copy-start
  101.6 10.7 %convolution_convert_fusion.1 = bf16[1024,640]{1,0:T(8,128)(2,1)S(1)} fusion(bf16[1024,4096]{1,0:T(8,128)(2,1)} %bitcast.151, bf16[4096,640]{1,0:T(8,128)(2,1)} %bitcast.153), kind=kOutput, calls=%fused_computation.15 | convolution fusion | flops 5369364480 | bytes 14942208 | tf_op jit(solution)/shard_map/dot_general | solution.py:380
  112.4 0.8 copy.36
  113.1 0.3 collective-permute-start
  113.4 0.8 fusion.22
  114.2 0.7 add_compare_fusion
  114.8 0.0 copy-done.1
  114.8 0.6 fusion.46
  115.4 0.0 copy-done
  115.4 1.5 slice_bitcast_fusion
  116.9 0.9 fusion.45
  117.8 1.2 broadcast_and_fusion
  118.9 1.2 maximum_bitcast_fusion.2
  120.2 0.7 dynamic-slice_bitcast_fusion.1
  121.0 0.1 copy.37
  121.2 0.2 copy.20
  121.4 0.9 pad_maximum_fusion.1.a_ref
  122.3 0.0 collective-permute-done
  122.3 1.2 fusion.2
  123.5 0.1 broadcast_maximum_fusion.1
  123.6 1.4 fusion
  125.0 0.1 exponential_add_fusion.1
  125.0 2.9 fusion.6
  127.9 1.6 copy.22
  129.5 1.1 fusion.19
  130.6 51.3 %mix1.1 = (bf16[1024,1024]{1,0:T(8,128)(2,1)}, bf16[1024,1024]{1,0:T(8,128)(2,1)}) custom-call(bf16[1024,256]{1,0:T(8,128)(2,1)} %bitcast.135, bf16[1024,512]{1,0:T(8,128)(2,1)} %get-tuple-element.22.o_ref), custom_call_target="tpu_custom_call" | custom-call | tf_op jit(solution)/shard_map/mix1/pallas_call | solution.py:238
  181.9 6.5 %fusion.47 = f32[1024,1024]{1,0:T(8,128)} fusion(bf16[1024,1024]{1,0:T(8,128)(2,1)} %get-tuple-element.15, bf16[1024,1024]{1,0:T(8,128)(2,1)} %get-tuple-element.16), kind=kOutput, calls=%fused_computation.98 | convolution fusion | flops 2147483648 | bytes 8388608 | tf_op jit(solution)/shard_map/dot_general | solution.py:410
  188.4 28.6 %settle2.1 = bf16[4,64,1024]{2,1,0:T(8,128)(2,1)} custom-call(f32[4,4,64,1024]{3,2,1,0:T(8,128)} %bitcast.130), custom_call_target="tpu_custom_call" | custom-call | tf_op jit(solution)/shard_map/settle2/pallas_call | solution.py:315
  217.1 1.1 convert_bitcast_fusion.1
  218.2 1.2 fusion.16
  219.5 0.1 copy.40
  219.6 1.0 multiply_convert_fusion.x_ref
  220.6 96.9 %gather3.1 = (bf16[4,4,64,4096]{3,2,1,0:T(8,128)(2,1)}, bf16[4,2,512,640]{3,2,1,0:T(8,128)(2,1)}) custom-call(bf16[64,4096]{1,0:T(8,128)(2,1)} %multiply_convert_fusion.x_ref, bf16[2,512,1024]{2,1,0:T(8,128)(2,1)} %q_ref.3, bf16[2,512,1024]{2,1,0:T(8,128)(2,1)} %g_ref.3, bf16[4,512,128]{2,1,0:T(8,128)(2,1)} %pad_maximum_fusion.1.a_ref), custom_call_target="tpu_custom_call" | custom-call | tf_op jit(solution)/shard_map/gather3/pallas_call | solution.py:183
  317.5 0.0 copy-start.2
  317.5 10.6 %convolution_convert_fusion = bf16[1024,640]{1,0:T(8,128)(2,1)S(1)} fusion(bf16[1024,4096]{1,0:T(8,128)(2,1)} %bitcast.150, bf16[4096,640]{1,0:T(8,128)(2,1)} %bitcast.152), kind=kOutput, calls=%fused_computation.14 | convolution fusion | flops 5369364480 | bytes 14942208 | tf_op jit(solution)/shard_map/dot_general | solution.py:380
  328.1 0.1 copy.38
  328.3 0.5 collective-permute-start.1
  328.8 0.0 copy-done.2
  328.8 0.1 dynamic-slice_bitcast_fusion
  328.9 0.2 copy.26
  329.1 0.1 copy.39
  329.3 2.9 collective-permute-done.1
  332.2 1.2 fusion.3
  333.4 0.1 broadcast_maximum_fusion
  333.5 1.4 fusion.1
  334.9 0.1 exponential_add_fusion
  334.9 2.9 fusion.4
  337.8 1.6 copy.28
  339.4 1.1 fusion.18
  340.5 49.9 %mix4.1 = (bf16[1024,1024]{1,0:T(8,128)(2,1)}, bf16[1024,1024]{1,0:T(8,128)(2,1)}) custom-call(bf16[1024,256]{1,0:T(8,128)(2,1)} %bitcast.134, bf16[1024,512]{1,0:T(8,128)(2,1)} %get-tuple-element.21.o_ref), custom_call_target="tpu_custom_call" | custom-call | tf_op jit(solution)/shard_map/mix4/pallas_call | solution.py:238
  390.4 6.5 %fusion.48 = f32[1024,1024]{1,0:T(8,128)} fusion(bf16[1024,1024]{1,0:T(8,128)(2,1)} %get-tuple-element.19, bf16[1024,1024]{1,0:T(8,128)(2,1)} %get-tuple-element.20), kind=kOutput, calls=%fused_computation.99 | convolution fusion | flops 2147483648 | bytes 8388608 | tf_op jit(solution)/shard_map/dot_general | solution.py:410
  396.9 28.3 %settle5.1 = bf16[4,64,1024]{2,1,0:T(8,128)(2,1)} custom-call(f32[4,4,64,1024]{3,2,1,0:T(8,128)} %bitcast.131), custom_call_target="tpu_custom_call" | custom-call | tf_op jit(solution)/shard_map/settle5/pallas_call | solution.py:315
  425.3 1.1 convert_bitcast_fusion
  426.4 1.2 fusion.17
  427.7 0.1 copy.41
  427.8 1.1 multiply_multiply_fusion
  (14 shorter events, 0.3 us)
Async XLA Ops:
  101.5 13.3 %copy-start.1 = (f32[2,64]{1,0:T(2,128)S(1)}, f32[2,64]{1,0:T(2,128)}, u32[]{:S(2)}) copy-start(f32[2,64]{1,0:T(2,128)} %param.14) | copy-start | bytes 1540
  101.6 13.9 %copy-start = (bf16[2,1024,512]{2,1,0:T(8,128)(2,1)S(1)}, bf16[2,1024,512]{2,1,0:T(8,128)(2,1)}, u32[]{:S(2)}) copy-start(bf16[2,1024,512]{2,1,0:T(8,128)(2,1)} %param.13) | copy-start | bytes 6291460
  113.1 9.1 %collective-permute-start = (bf16[4,128,128]{1,2,0:T(8,128)(2,1)}, bf16[4,128,128]{1,2,0:T(8,128)(2,1)S(1)}, u32[]{:S(2)}, u32[]{:S(2)}) collective-permute-start(bf16[4,128,128]{1,2,0:T(8,128)(2,1)} %copy.36), channel_id=1, source_target_pairs={{0,4},{4,0},{8,12},{12,8},{16,20},{20,16},{24,28},{28,24},{1,5},{5... | collective-permute-start | bytes 393224 | tf_op jit(solution)/shard_map/ppermute | solution.py:383
  317.5 11.3 %copy-start.2 = (f32[1,64]{1,0:T(1,128)S(1)}, f32[1,64]{1,0:T(1,128)}, u32[]{:S(2)}) copy-start(f32[1,64]{1,0:T(1,128)} %get-tuple-element.33) | copy-start | bytes 772
  328.3 3.9 collective-permute-start.1

commit v4 on v3

--- a/solution.py
+++ b/solution.py
@@ -156,11 +156,10 @@
     own_rows.start()
     for src, dst in pieces(z):
         pltpu.make_async_copy(src, dst, own_sem.at[1]).start()
-    send_w(1)
+    for step in range(1, nz):
+        send_w(step)
     for step in range(1, nz):
         visits(z, nz, step, arrive)
-        if step + 1 < nz:
-            send_w(step + 1)
         w_arrive(step)
     for step in range(nz):
         visits(z, nz, step, from_y)

time: 430 us -> 428 us (level)
    pallas_call x2, Pallas kernels: 101 us -> 67.5 us  [mix(): pl.pallas_call(functools.partial(mix_kernel, nz, nx, nc), out_shape=(jax....]
    pallas_call x2, Pallas kernels: 194 us -> 225 us  [gather(): pl.pallas_call(functools.partial(gather_kernel, nz, nx, ny, nc, layer), o...]
where the time goes in v4:
time: 428 us; the launch traced here: 427 us
  Pallas kernels  350 us (82%)
  matrix products  42.5 us (10%)
  other arithmetic  18 us (4%)
  local copies, waits for them, and re-layouts  12.7 us (3%)
    pallas_call x2, Pallas kernels, gather(): pl.pallas_call(functools.partial(gather_kernel, nz, nx, ny, nc, layer), o...  225 us
    pallas_call x2, Pallas kernels, mix(): pl.pallas_call(functools.partial(mix_kernel, nz, nx, nc), out_shape=(jax....  67.5 us
    pallas_call x2, Pallas kernels, settle(): pl.pallas_call(functools.partial(settle_kernel, nz, nx, ny, nc), out_shap...  58 us
    dot_general x2, matrix products, per_device(): jnp.dot(rows, joined, preferred_element_type=jnp.float32)  21.4 us
    dot_general x2, matrix products, per_device(): jnp.dot(hidden, out_cols, preferred_element_type=jnp.float32)  13 us
  transfers between devices with their start and end apart: 2, of which 1 were waited for; matrix products, arithmetic and copies ran while one was open for 2% of the time, Pallas kernels for 0%

profile of v4, /device:TPU:9, one launch (start us, length us, event | category | flops | bytes accessed | tf_op | source)
XLA Modules:
  0.0 427.2 jit_solution(11948084832210776879)
XLA Ops:
  0.0 1.9 slice_bitcast_fusion.5
  1.9 1.9 slice_bitcast_fusion.4
  3.8 0.1 maximum_bitcast_fusion
  3.9 0.8 pad_maximum_fusion.a_ref
  4.8 112.7 %gather0.1 = (bf16[4,4,64,4096]{3,2,1,0:T(8,128)(2,1)}, bf16[4,2,512,640]{3,2,1,0:T(8,128)(2,1)}) custom-call(bf16[64,4096]{1,0:T(8,128)(2,1)} %x_ref.1, bf16[2,512,1024]{2,1,0:T(8,128)(2,1)} %q_ref.3, bf16[2,512,1024]{2,1,0:T(8,128)(2,1)} %g_ref.3, bf16[4,512,128]{2,1,0:T(8,128)(2,1)} %pad_maximum_fusion.a_ref), custom_call_target="tpu_custom_call" | custom-call | tf_op jit(solution)/shard_map/gather0/pallas_call | solution.py:182
  117.5 0.0 copy-start.1
  117.5 0.0 copy-start
  117.5 10.7 %convolution_convert_fusion.1 = bf16[1024,640]{1,0:T(8,128)(2,1)S(1)} fusion(bf16[1024,4096]{1,0:T(8,128)(2,1)} %bitcast.151, bf16[4096,640]{1,0:T(8,128)(2,1)} %bitcast.153), kind=kOutput, calls=%fused_computation.15 | convolution fusion | flops 5369364480 | bytes 14942208 | tf_op jit(solution)/shard_map/dot_general | solution.py:379
  128.3 0.8 copy.36
  129.0 0.3 collective-permute-start
  129.3 0.8 fusion.22
  130.1 0.7 add_compare_fusion
  130.7 0.0 copy-done.1
  130.7 0.6 fusion.46
  131.3 0.0 copy-done
  131.3 1.5 slice_bitcast_fusion
  132.8 0.9 fusion.45
  133.7 1.2 broadcast_and_fusion
  134.9 1.2 maximum_bitcast_fusion.2
  136.1 0.7 dynamic-slice_bitcast_fusion.1
  136.9 0.1 copy.37
  137.1 0.2 copy.20
  137.3 0.9 pad_maximum_fusion.1.a_ref
  138.2 0.0 collective-permute-done
  138.2 1.2 fusion.2
  139.4 0.1 broadcast_maximum_fusion.1
  139.5 1.4 fusion
  140.9 0.1 exponential_add_fusion.1
  140.9 2.9 fusion.6
  143.8 1.6 copy.22
  145.4 1.1 fusion.19
  146.5 34.4 %mix1.1 = (bf16[1024,1024]{1,0:T(8,128)(2,1)}, bf16[1024,1024]{1,0:T(8,128)(2,1)}) custom-call(bf16[1024,256]{1,0:T(8,128)(2,1)} %bitcast.135, bf16[1024,512]{1,0:T(8,128)(2,1)} %get-tuple-element.22.o_ref), custom_call_target="tpu_custom_call" | custom-call | tf_op jit(solution)/shard_map/mix1/pallas_call | solution.py:237
  180.9 6.5 %fusion.47 = f32[1024,1024]{1,0:T(8,128)} fusion(bf16[1024,1024]{1,0:T(8,128)(2,1)} %get-tuple-element.15, bf16[1024,1024]{1,0:T(8,128)(2,1)} %get-tuple-element.16), kind=kOutput, calls=%fused_computation.98 | convolution fusion | flops 2147483648 | bytes 8388608 | tf_op jit(solution)/shard_map/dot_general | solution.py:409
  187.4 28.9 %settle2.1 = bf16[4,64,1024]{2,1,0:T(8,128)(2,1)} custom-call(f32[4,4,64,1024]{3,2,1,0:T(8,128)} %bitcast.130), custom_call_target="tpu_custom_call" | custom-call | tf_op jit(solution)/shard_map/settle2/pallas_call | solution.py:314
  216.3 1.1 convert_bitcast_fusion.1
  217.4 1.2 fusion.16
  218.7 0.1 copy.40
  218.8 1.0 multiply_convert_fusion.x_ref
  219.8 112.0 %gather3.1 = (bf16[4,4,64,4096]{3,2,1,0:T(8,128)(2,1)}, bf16[4,2,512,640]{3,2,1,0:T(8,128)(2,1)}) custom-call(bf16[64,4096]{1,0:T(8,128)(2,1)} %multiply_convert_fusion.x_ref, bf16[2,512,1024]{2,1,0:T(8,128)(2,1)} %q_ref.3, bf16[2,512,1024]{2,1,0:T(8,128)(2,1)} %g_ref.3, bf16[4,512,128]{2,1,0:T(8,128)(2,1)} %pad_maximum_fusion.1.a_ref), custom_call_target="tpu_custom_call" | custom-call | tf_op jit(solution)/shard_map/gather3/pallas_call | solution.py:182
  331.8 0.0 copy-start.2
  331.8 10.6 %convolution_convert_fusion = bf16[1024,640]{1,0:T(8,128)(2,1)S(1)} fusion(bf16[1024,4096]{1,0:T(8,128)(2,1)} %bitcast.150, bf16[4096,640]{1,0:T(8,128)(2,1)} %bitcast.152), kind=kOutput, calls=%fused_computation.14 | convolution fusion | flops 5369364480 | bytes 14942208 | tf_op jit(solution)/shard_map/dot_general | solution.py:379
  342.5 0.1 copy.38
  342.6 0.4 collective-permute-start.1
  343.0 0.0 copy-done.2
  343.0 0.1 dynamic-slice_bitcast_fusion
  343.2 0.2 copy.26
  343.4 0.1 copy.39
  343.5 2.9 collective-permute-done.1
  346.5 1.2 fusion.3
  347.7 0.1 broadcast_maximum_fusion
  347.8 1.4 fusion.1
  349.2 0.1 exponential_add_fusion
  349.3 2.9 fusion.4
  352.1 1.6 copy.28
  353.7 1.1 fusion.18
  354.8 33.1 %mix4.1 = (bf16[1024,1024]{1,0:T(8,128)(2,1)}, bf16[1024,1024]{1,0:T(8,128)(2,1)}) custom-call(bf16[1024,256]{1,0:T(8,128)(2,1)} %bitcast.134, bf16[1024,512]{1,0:T(8,128)(2,1)} %get-tuple-element.21.o_ref), custom_call_target="tpu_custom_call" | custom-call | tf_op jit(solution)/shard_map/mix4/pallas_call | solution.py:237
  387.9 6.5 %fusion.48 = f32[1024,1024]{1,0:T(8,128)} fusion(bf16[1024,1024]{1,0:T(8,128)(2,1)} %get-tuple-element.19, bf16[1024,1024]{1,0:T(8,128)(2,1)} %get-tuple-element.20), kind=kOutput, calls=%fused_computation.99 | convolution fusion | flops 2147483648 | bytes 8388608 | tf_op jit(solution)/shard_map/dot_general | solution.py:409
  394.4 29.1 %settle5.1 = bf16[4,64,1024]{2,1,0:T(8,128)(2,1)} custom-call(f32[4,4,64,1024]{3,2,1,0:T(8,128)} %bitcast.131), custom_call_target="tpu_custom_call" | custom-call | tf_op jit(solution)/shard_map/settle5/pallas_call | solution.py:314
  423.5 1.1 convert_bitcast_fusion
  424.7 1.2 fusion.17
  425.9 0.1 copy.41
  426.1 1.1 multiply_multiply_fusion
  (14 shorter events, 0.3 us)
Async XLA Ops:
  117.5 13.3 %copy-start.1 = (f32[2,64]{1,0:T(2,128)S(1)}, f32[2,64]{1,0:T(2,128)}, u32[]{:S(2)}) copy-start(f32[2,64]{1,0:T(2,128)} %param.14) | copy-start | bytes 1540
  117.5 13.9 %copy-start = (bf16[2,1024,512]{2,1,0:T(8,128)(2,1)S(1)}, bf16[2,1024,512]{2,1,0:T(8,128)(2,1)}, u32[]{:S(2)}) copy-start(bf16[2,1024,512]{2,1,0:T(8,128)(2,1)} %param.13) | copy-start | bytes 6291460
  129.0 9.1 %collective-permute-start = (bf16[4,128,128]{1,2,0:T(8,128)(2,1)}, bf16[4,128,128]{1,2,0:T(8,128)(2,1)S(1)}, u32[]{:S(2)}, u32[]{:S(2)}) collective-permute-start(bf16[4,128,128]{1,2,0:T(8,128)(2,1)} %copy.36), channel_id=1, source_target_pairs={{0,4},{4,0},{8,12},{12,8},{16,20},{20,16},{24,28},{28,24},{1,5},{5... | collective-permute-start | bytes 393224 | tf_op jit(solution)/shard_map/ppermute | solution.py:382
  331.8 11.2 %copy-start.2 = (f32[1,64]{1,0:T(1,128)S(1)}, f32[1,64]{1,0:T(1,128)}, u32[]{:S(2)}) copy-start(f32[1,64]{1,0:T(1,128)} %get-tuple-element.33) | copy-start | bytes 772
  342.6 3.9 collective-permute-start.1
